TPU v7x, 32 devices: a whole 2x2x4 slice. The times are simulated.
32 devices in a mesh: dp: 4 (over y, x), kv: 4 (over z), tp: 2 (over core).
Axes of the slice: x: 2, y: 2, z: 4, core: 2. Of those that a mesh axis runs over, the one named last changes fastest.
Arguments:
- tokens: bfloat16 [1024, 2048], P(('dp', 'kv', 'tp')), may hold values from -6 to 6
- norm_gain: float32 [2048], replicated, may hold values from 0.1 to 1.9
- gate_proj: bfloat16 [2048, 4096], P(None, ('kv', 'tp')), may hold values from -0.125 to 0.125
- inner_proj: bfloat16 [2048, 4096], P(None, ('kv', 'tp')), may hold values from -0.125 to 0.125
- write_proj: bfloat16 [2048, 1024], P(None, ('kv', 'tp')), may hold values from -0.125 to 0.125
- read_proj: bfloat16 [2048, 1024], P(None, ('kv', 'tp')), may hold values from -0.125 to 0.125
- step_proj: bfloat16 [2048, 64], replicated, may hold values from -0.125 to 0.125
- step_bias: float32 [64], replicated, may hold values from -3 to 0
- decay_log: float32 [64], replicated, may hold values from -5 to 0.7
- skip_gain: float32 [64], replicated, may hold values from 0.25 to 4
- conv_inner: bfloat16 [4, 4096], replicated, may hold values from -3 to 3
- conv_write: bfloat16 [4, 1024], replicated, may hold values from -3 to 3
- conv_read: bfloat16 [4, 1024], replicated, may hold values from -3 to 3
- out_gain: float32 [4096], replicated, may hold values from 0.1 to 1.9
- out_proj: bfloat16 [4096, 2048], P(('kv', 'tp')), may hold values from -0.09375 to 0.09375
- saved_state: float32 [256, 64, 64, 128], P('dp', ('kv', 'tp')), may hold values from -1.75 to 1.75
- inner_history: bfloat16 [256, 7, 4096], P('dp', None, ('kv', 'tp')), may hold values from -6 to 6
- write_history: bfloat16 [256, 7, 1024], P('dp', None, ('kv', 'tp')), may hold values from -6 to 6
- read_history: bfloat16 [256, 7, 1024], P('dp', None, ('kv', 'tp')), may hold values from -6 to 6
- last_steps: float32 [256, 4, 64], P('dp', None, ('kv', 'tp')), may hold values from 0.02 to 1
- accepted: int32 [256], P('dp'), may hold values from 0 to 4
Outputs:
- mixed: bfloat16 [1024, 2048], P(('dp', 'kv', 'tp'))
- base_state: float32 [256, 64, 64, 128], P('dp', ('kv', 'tp'))
All inputs are finite; a program needn't handle non-finite values.
Results may differ from a plain program's by a relative error of at most 0.014.
Values may be sent and summed in bfloat16 or wider, within the bound.
A program may use at most 128 MiB of HBM per device.

v0:
```python
import functools

import jax
import jax.numpy as jnp
from jax import lax
from jax.experimental import pallas as pl
from jax.experimental.pallas import tpu as pltpu
from jax.sharding import PartitionSpec as P

GROUPS = 8
EPSILON = 0.1
BLOCK = 8
highest = lax.Precision.HIGHEST


def swapped(value, axis, stride):
    mask = 2**stride
    pairs = [(source, source ^ mask) for source in range(lax.axis_size(axis))]
    return lax.ppermute(value, axis, pairs)


def mix_kernel(
    rank_ref,
    acc_ref,
    steps_ref,
    last_ref,
    par_ref,
    gate_ref,
    inner_ref,
    write_ref,
    read_ref,
    hist_inner_ref,
    hist_write_ref,
    hist_read_ref,
    taps_inner_ref,
    taps_write_ref,
    taps_read_ref,
    gain_ref,
    expand_ref,
    state_ref,
    un_ref,
    sq_ref,
    base_ref,
):
    f32 = jnp.float32
    props = steps_ref.shape[0]
    heads = last_ref.shape[2]
    cols = inner_ref.shape[2]
    states = write_ref.shape[2]
    head_dim = cols // heads
    hist = hist_inner_ref.shape[0]
    width = taps_inner_ref.shape[0]
    acc = acc_ref[...]

    def silu(x):
        return x / (1.0 + jnp.exp(-x))

    def slabs(ref):
        return [ref[k].astype(f32) for k in range(ref.shape[0])]

    round_bf = lambda x: x.astype(jnp.bfloat16).astype(f32)

    def conv(rows, taps_ref):
        taps = taps_ref[...].astype(f32)
        res = []
        for r in range(len(rows) - width + 1):
            v = taps[0:1] * rows[r]
            for k in range(1, width):
                v = v + taps[k : k + 1] * rows[r + k]
            res.append(silu(v))
        return res

    def current(h, new_ref):
        where_at = jnp.broadcast_to(acc, h[0].shape)
        rows = []
        for k in range(width - 1):
            r = h[k]
            for v in range(1, hist - width + 2):
                r = jnp.where(where_at == v, h[k + v], r)
            rows.append(r)
        return rows + [round_bf(x) for x in slabs(new_ref)]

    h_inner = slabs(hist_inner_ref)
    inner_old = conv(h_inner, taps_inner_ref)
    inner_new = conv(current(h_inner, inner_ref), taps_inner_ref)
    h_write = slabs(hist_write_ref)
    write_old = [round_bf(x) for x in conv(h_write, taps_write_ref)]
    write_new = [round_bf(x) for x in conv(current(h_write, write_ref), taps_write_ref)]
    read_new = [round_bf(x) for x in conv(current(slabs(hist_read_ref), read_ref), taps_read_ref)]

    bias = par_ref[0:1]
    rate = -jnp.exp(par_ref[1:2])
    skip = par_ref[2:3]
    acc_h = jnp.broadcast_to(acc, (BLOCK, heads))
    masks = [jnp.where(acc_h > t, 1.0, 0.0) for t in range(props)]
    logs = [rate * last_ref[t] * masks[t] for t in range(props)]
    coefs = [None] * props
    tail = jnp.zeros((BLOCK, heads), f32)
    for t in reversed(range(props)):
        coefs[t] = masks[t] * jnp.exp(tail) * last_ref[t]
        tail = tail + logs[t]
    decay = jnp.exp(tail)
    step = []
    for t in range(props):
        x = steps_ref[t][:, :heads] + bias
        step.append(jnp.maximum(x, 0.0) + jnp.log1p(jnp.exp(-jnp.abs(x))))
    cums = []
    for t in range(props):
        cums.append(rate * step[t] + (cums[-1] if cums else 0.0))
    where_of = {}
    for i in range(props):
        for j in range(i + 1):
            score = jnp.sum(read_new[i] * write_new[j], axis=-1, keepdims=True)
            c = jnp.exp(cums[i] - cums[j]) * step[j] * score
            if i == j:
                c = c + skip
            where_of[(i, j)] = len(coefs)
            coefs.append(c)
    first_cum = len(coefs)
    for i in range(props):
        coefs.append(jnp.exp(cums[i]))
    wide = jnp.dot(
        jnp.concatenate(coefs, axis=0),
        expand_ref[...],
        precision=highest,
        preferred_element_type=f32,
    )

    def at(k):
        return wide[k * BLOCK : (k + 1) * BLOCK]

    left = jnp.concatenate([at(t) * inner_old[t] for t in range(props)], axis=0)
    high = round_bf(left)
    both = jnp.concatenate([high, left - high], axis=0)
    turned = jnp.transpose(both).astype(jnp.bfloat16)
    write_all = jnp.concatenate(write_old + write_old, axis=0)
    read_all = jnp.concatenate(read_new, axis=0)
    seq_w = lax.broadcasted_iota(jnp.int32, write_all.shape, 0) % BLOCK
    seq_r = lax.broadcasted_iota(jnp.int32, read_all.shape, 0) % BLOCK
    carried = jnp.zeros((props * BLOCK, cols), f32)
    for s in range(BLOCK):
        right = jnp.where(seq_w == s, write_all, 0.0).astype(jnp.bfloat16)
        update = jnp.dot(turned, right, preferred_element_type=f32)
        parts = []
        for h in range(heads):
            lo, hi = h * head_dim, (h + 1) * head_dim
            d = jnp.broadcast_to(decay[s : s + 1, h : h + 1], (head_dim, states))
            new = d * state_ref[s, lo:hi, :] + update[lo:hi]
            base_ref[s, lo:hi, :] = new
            parts.append(new.astype(jnp.bfloat16))
        asked = jnp.where(seq_r == s, read_all, 0.0).astype(jnp.bfloat16)
        carried = carried + lax.dot_general(
            asked,
            jnp.concatenate(parts, axis=0),
            (((1,), (1,)), ((), ())),
            preferred_element_type=f32,
        )
    for i in range(props):
        y = at(first_cum + i) * carried[i * BLOCK : (i + 1) * BLOCK]
        for j in range(i + 1):
            y = y + at(where_of[(i, j)]) * inner_new[j]
        g = y * silu(gate_ref[i].astype(f32))
        sq_ref[i] = jnp.broadcast_to(jnp.sum(g * g, axis=-1, keepdims=True), sq_ref.shape[1:])
        un_ref[i] = (g * gain_ref[...]).astype(un_ref.dtype)


def mix(rank, group, acc, last, par, gate, inner, small, hi, hw, hr, ci, cw, cr, gain, state):
    props, seqs, heads = last.shape
    cols, states = state.shape[1], state.shape[2]
    expand = (jnp.arange(cols)[None, :] // (cols // heads) == jnp.arange(heads)[:, None]).astype(
        jnp.float32
    )
    hist = hi.shape[0]
    width = ci.shape[0]

    def slab(lead, last_dim):
        return pl.BlockSpec((lead, BLOCK, last_dim), lambda g, r: (0, g, 0))

    def piece(which):
        return pl.BlockSpec((props, BLOCK, states), lambda g, r: (0, g, which))

    def own(rows, last_dim, which):
        return pl.BlockSpec((rows, last_dim), lambda g, r: (0, r[which]))

    state_spec = pl.BlockSpec((BLOCK, cols, states), lambda g, r: (g, 0, 0))
    return pl.pallas_call(
        mix_kernel,
        grid_spec=pltpu.PrefetchScalarGridSpec(
            num_scalar_prefetch=1,
            grid=(seqs // BLOCK,),
            in_specs=[
                pl.BlockSpec((BLOCK, 1), lambda g, r: (g, 0)),
                piece(2),
                slab(props, heads),
                pl.BlockSpec(par.shape, lambda g, r: (0, 0)),
                slab(props, cols),
                slab(props, cols),
                piece(0),
                piece(1),
                slab(hist, cols),
                slab(hist, states),
                slab(hist, states),
                own(width, cols, 0),
                own(width, states, 1),
                own(width, states, 1),
                own(1, cols, 0),
                pl.BlockSpec(expand.shape, lambda g, r: (0, 0)),
                state_spec,
            ],
            out_specs=[slab(props, cols), slab(props, 128), state_spec],
        ),
        out_shape=[
            jax.ShapeDtypeStruct((props, seqs, cols), jnp.bfloat16),
            jax.ShapeDtypeStruct((props, seqs, 128), jnp.float32),
            jax.ShapeDtypeStruct(state.shape, jnp.float32),
        ],
        compiler_params=pltpu.CompilerParams(
            dimension_semantics=("arbitrary",), vmem_limit_bytes=48 * 1024 * 1024
        ),
        name="mix",
    )(
        jnp.stack([rank, group]).astype(jnp.int32),
        acc, small, last, par, gate, inner, small, small, hi, hw, hr, ci, cw, cr, gain, expand, state,
    )


MESH = pl.DeviceIdType.MESH
CHUNKS = 2


def remote(src, dst, send, recv, where):
    return pltpu.make_async_remote_copy(
        src_ref=src, dst_ref=dst, send_sem=send, recv_sem=recv, device_id=where, device_id_type=MESH
    )


def gather_kernel(n, own_ref, out_ref, rs, rr, ls, lr, fs, fr, local_sem):
    k = lax.axis_index("kv")
    t = lax.axis_index("tp")
    right = {"kv": lax.rem(k + 1, n)}
    left = {"kv": lax.rem(k + n - 1, n)}
    partner = {"tp": 1 - t}
    span = own_ref.shape[1] // CHUNKS
    barrier = pltpu.get_barrier_semaphore()
    pl.semaphore_signal(barrier, inc=1, device_id=partner, device_id_type=MESH)

    @pl.when(k < n - 1)
    def _():
        pl.semaphore_signal(barrier, inc=1, device_id=right, device_id_type=MESH)

    @pl.when(k > 0)
    def _():
        pl.semaphore_signal(barrier, inc=1, device_id=left, device_id_type=MESH)

    inner = (k > 0) & (k < n - 1)

    @pl.when(inner)
    def _():
        pl.semaphore_wait(barrier, 3)

    @pl.when(jnp.logical_not(inner))
    def _():
        pl.semaphore_wait(barrier, 2)

    def view(j, c):
        return out_ref.at[j, t, :, pl.ds(c * span, span)]

    def own(c):
        return own_ref.at[:, pl.ds(c * span, span)]

    def to_right(s, c):
        j = jnp.maximum(k - s, 0)
        return remote(own(c) if s == 0 else view(j, c), view(j, c), rs.at[s, c], rr.at[s, c], right)

    def to_left(s, c):
        j = jnp.minimum(k + s, n - 1)
        return remote(own(c) if s == 0 else view(j, c), view(j, c), ls.at[s, c], lr.at[s, c], left)

    def across(j, c, mine=False):
        return remote(own(c) if mine else view(j, c), view(j, c), fs.at[j, c], fr.at[j, c], partner)

    for s in range(n - 1):
        for c in range(CHUNKS):
            if s > 0:
                @pl.when(k - s >= 0)
                def _():
                    to_right(s - 1, c).wait_recv()

                @pl.when(k + s < n)
                def _():
                    to_left(s - 1, c).wait_recv()

            @pl.when((k - s >= 0) & (k < n - 1))
            def _():
                to_right(s, c).start()

            @pl.when((k + s < n) & (k > 0))
            def _():
                to_left(s, c).start()

            if s == 0:
                across(k, c, True).start()
            else:
                @pl.when(k - s >= 0)
                def _():
                    across(k - s, c).start()

                @pl.when(k + s < n)
                def _():
                    across(k + s, c).start()
        if s == 0:
            local = pltpu.make_async_copy(own_ref, out_ref.at[k, t], local_sem)
            local.start()
            local.wait()
    s = n - 1
    for c in range(CHUNKS):
        @pl.when(k - s >= 0)
        def _():
            to_right(s - 1, c).wait_recv()
            across(k - s, c).start()

        @pl.when(k + s < n)
        def _():
            to_left(s - 1, c).wait_recv()
            across(k + s, c).start()
    for s in range(n - 1):
        for c in range(CHUNKS):
            @pl.when((k - s >= 0) & (k < n - 1))
            def _():
                to_right(s, c).wait_send()

            @pl.when((k + s < n) & (k > 0))
            def _():
                to_left(s, c).wait_send()
    for j in range(n):
        for c in range(CHUNKS):
            across(j, c).wait_send()
            remote(
                out_ref.at[j, 1 - t, :, pl.ds(c * span, span)],
                out_ref.at[j, 1 - t, :, pl.ds(c * span, span)],
                fs.at[j, c],
                fr.at[j, c],
                partner,
            ).wait_recv()


def gathered(own):
    n = lax.axis_size("kv")
    rows, cols = own.shape
    dma = pltpu.SemaphoreType.DMA
    out = pl.pallas_call(
        functools.partial(gather_kernel, n),
        out_shape=jax.ShapeDtypeStruct((n, 2, rows, cols), own.dtype),
        in_specs=[pl.BlockSpec(memory_space=pltpu.VMEM)],
        out_specs=pl.BlockSpec(memory_space=pltpu.VMEM),
        scratch_shapes=[dma((n - 1, CHUNKS))] * 4 + [dma((n, CHUNKS))] * 2 + [dma],
        compiler_params=pltpu.CompilerParams(
            collective_id=0, has_side_effects=True, vmem_limit_bytes=32 * 1024 * 1024
        ),
        name="gather",
    )(own)
    return out.reshape(n * 2 * rows, cols)


def scatter_kernel(
    n, part, sq, out, sqs, pbuf, rbuf, lbuf, rout, lout, ps, pr, rs, rr, ls, lr, ss, sr
):
    f32 = jnp.float32
    k = lax.axis_index("kv")
    t = lax.axis_index("tp")
    rank = k * 2 + t
    ranks = n * 2
    right = {"kv": lax.rem(k + 1, n)}
    left = {"kv": lax.rem(k + n - 1, n)}
    partner = {"tp": 1 - t}
    span = part.shape[3] // CHUNKS
    barrier = pltpu.get_barrier_semaphore()

    def peer(o):
        p = lax.rem(rank + o, ranks)
        return {"kv": p // 2, "tp": lax.rem(p, 2)}

    for o in range(1, ranks):
        pl.semaphore_signal(barrier, inc=1, device_id=peer(o), device_id_type=MESH)
    pl.semaphore_wait(barrier, ranks - 1)

    def cut(c):
        return pl.ds(c * span, span)

    def across(j, c):
        return remote(
            part.at[j, 1 - t, :, cut(c)], pbuf.at[j, :, cut(c)], ps.at[j, c], pr.at[j, c], partner
        )

    def to_right(d, c):
        return remote(
            rout.at[d, :, cut(c)], rbuf.at[d, :, cut(c)], rs.at[d, c], rr.at[d, c], right
        )

    def to_left(d, c):
        return remote(lout.at[d, :, cut(c)], lbuf.at[d, :, cut(c)], ls.at[d, c], lr.at[d, c], left)

    def square(o):
        p = lax.rem(rank + o, ranks)
        return remote(sq.at[p], sqs.at[rank], ss.at[o], sr.at[o], peer(o))

    low = k < n // 2
    for i in range(n):
        j = jnp.where(low, n - 1 - i, i)
        for c in range(CHUNKS):
            across(j, c).start()
    for o in range(1, ranks):
        square(o).start()
    sqs[rank] = sq[rank]

    def pair(j, c):
        across(j, c).wait_recv()
        return part[j, t, :, cut(c)].astype(f32) + pbuf[j, :, cut(c)].astype(f32)

    def rightward():
        for d in range(n - 1, 0, -1):
            for c in range(CHUNKS):
                @pl.when((k < d) & (k == 0))
                def _():
                    rout[d, :, cut(c)] = pair(d, c).astype(rout.dtype)
                    to_right(d, c).start()

                @pl.when((k < d) & (k > 0))
                def _():
                    value = pair(d, c)
                    to_right(d, c).wait_recv()
                    rout[d, :, cut(c)] = (value + rbuf[d, :, cut(c)].astype(f32)).astype(rout.dtype)
                    to_right(d, c).start()

    def leftward():
        for d in range(n - 1):
            for c in range(CHUNKS):
                @pl.when((k > d) & (k == n - 1))
                def _():
                    lout[d, :, cut(c)] = pair(d, c).astype(lout.dtype)
                    to_left(d, c).start()

                @pl.when((k > d) & (k < n - 1))
                def _():
                    value = pair(d, c)
                    to_left(d, c).wait_recv()
                    lout[d, :, cut(c)] = (value + lbuf[d, :, cut(c)].astype(f32)).astype(lout.dtype)
                    to_left(d, c).start()

    @pl.when(k < n // 2)
    def _():
        rightward()
        leftward()

    @pl.when(k >= n // 2)
    def _():
        leftward()
        rightward()

    for c in range(CHUNKS):
        out[:, cut(c)] = pair(k, c)

        @pl.when(k > 0)
        def _():
            to_right(k, c).wait_recv()
            out[:, cut(c)] += rbuf[k, :, cut(c)].astype(f32)

        @pl.when(k < n - 1)
        def _():
            to_left(k, c).wait_recv()
            out[:, cut(c)] += lbuf[k, :, cut(c)].astype(f32)

    for j in range(n):
        for c in range(CHUNKS):
            across(j, c).wait_send()

            @pl.when(k < j)
            def _():
                to_right(j, c).wait_send()

            @pl.when(k > j)
            def _():
                to_left(j, c).wait_send()
    for o in range(1, ranks):
        square(o).wait_send()
        source = lax.rem(rank + ranks - o, ranks)
        remote(sq.at[rank], sqs.at[source], ss.at[o], sr.at[o], peer(o)).wait_recv()


def scattered(partial_value, squares):
    n = lax.axis_size("kv")
    ranks = n * 2
    rows = partial_value.shape[0] // ranks
    cols = partial_value.shape[1]
    squares = jnp.pad(squares.reshape(ranks, 1, rows), ((0, 0), (0, 7), (0, 128 - rows)))
    dma = pltpu.SemaphoreType.DMA
    vmem = pl.BlockSpec(memory_space=pltpu.VMEM)
    kind = partial_value.dtype
    summed, sqs = pl.pallas_call(
        functools.partial(scatter_kernel, n),
        out_shape=[
            jax.ShapeDtypeStruct((rows, cols), jnp.float32),
            jax.ShapeDtypeStruct(squares.shape, jnp.float32),
        ],
        in_specs=[vmem, vmem],
        out_specs=[vmem, vmem],
        scratch_shapes=[pltpu.VMEM((n, rows, cols), kind)] * 5
        + [dma((n, CHUNKS))] * 6
        + [dma((ranks,))] * 2,
        compiler_params=pltpu.CompilerParams(
            collective_id=1, has_side_effects=True, vmem_limit_bytes=32 * 1024 * 1024
        ),
        name="scatter",
    )(partial_value.reshape(n, 2, rows, cols), squares)
    return summed, jnp.sum(sqs[:, 0, :rows], axis=0)


def body(
    tokens,
    norm_gain,
    gate_proj,
    inner_proj,
    write_proj,
    read_proj,
    step_proj,
    step_bias,
    decay_log,
    skip_gain,
    conv_inner,
    conv_write,
    conv_read,
    out_gain,
    out_proj,
    saved_state,
    inner_history,
    write_history,
    read_history,
    last_steps,
    accepted,
):
    device_rank = lax.axis_index(("kv", "tp"))
    seq_count = saved_state.shape[0]
    local_heads = saved_state.shape[1]
    head_dim = saved_state.shape[2]
    proposals = last_steps.shape[1]
    inner_cols = inner_proj.shape[1]
    state_cols = write_proj.shape[1]
    token_count = tokens.shape[0]
    own_rows = tokens.astype(jnp.float32)
    normed_own = (
        own_rows
        * lax.rsqrt(jnp.mean(own_rows * own_rows, axis=-1, keepdims=True) + EPSILON)
        * norm_gain
    ).astype(jnp.bfloat16)
    normed = gathered(normed_own)
    normed = normed.reshape(seq_count, proposals, -1).transpose(1, 0, 2)
    normed = normed.reshape(proposals * seq_count, -1)

    def project(weight):
        out = jnp.dot(normed, weight, preferred_element_type=jnp.float32)
        return out.reshape(proposals, seq_count, -1)

    gate_rows = project(gate_proj).astype(jnp.bfloat16)
    inner_rows = project(inner_proj).astype(jnp.bfloat16)
    first_head = device_rank * local_heads
    state_cols = write_proj.shape[1]
    states = saved_state.shape[3]
    step_local = lax.dynamic_slice_in_dim(step_proj, first_head, local_heads, 1)
    step_local = jnp.pad(step_local, ((0, 0), (0, states - local_heads)))
    small = project(jnp.concatenate([write_proj, read_proj, step_local], axis=1))
    par = lax.dynamic_slice_in_dim(
        jnp.stack([step_bias, decay_log, skip_gain]), first_head, local_heads, 1
    )
    slab = lambda x: x.transpose(1, 0, 2)
    hist_inner, hist_write, hist_read = slab(inner_history), slab(write_history), slab(read_history)
    group_span = lax.axis_size("kv") * lax.axis_size("tp") // GROUPS
    if group_span >= 2:
        write_rows = small[:, :, :state_cols].astype(jnp.bfloat16)
        read_rows = small[:, :, state_cols : 2 * state_cols].astype(jnp.bfloat16)
        pieces = (write_rows, read_rows, hist_write, hist_read)
        pieces = tuple(lax.all_gather(x, "tp", axis=2, tiled=True) for x in pieces)
        kv_rank = lax.axis_index("kv")
        bit_count = (group_span // lax.axis_size("tp")).bit_length() - 1
        for bit in range(bit_count):
            partner = swapped(pieces, "kv", bit)
            lower = jnp.bitwise_and(jnp.right_shift(kv_rank, bit), 1) == 0
            pieces = tuple(
                jnp.where(
                    lower,
                    jnp.concatenate([mine, theirs], axis=2),
                    jnp.concatenate([theirs, mine], axis=2),
                )
                for mine, theirs in zip(pieces, partner)
            )
        write_rows, read_rows, hist_write, hist_read = pieces
        small = jnp.concatenate(
            [
                write_rows.astype(jnp.float32),
                read_rows.astype(jnp.float32),
                small[:, :, 2 * state_cols :],
            ],
            axis=2,
        )
    unscaled, squares, base_state = mix(
        device_rank,
        device_rank // group_span,
        accepted[:, None],
        slab(last_steps),
        par,
        gate_rows,
        inner_rows,
        small,
        hist_inner,
        hist_write,
        hist_read,
        conv_inner,
        conv_write,
        conv_read,
        out_gain[None, :],
        saved_state.reshape(seq_count, local_heads * head_dim, -1),
    )
    base_state = base_state.reshape(saved_state.shape)
    unscaled = unscaled.transpose(1, 0, 2).reshape(seq_count * proposals, inner_cols)
    partial_value = jnp.dot(unscaled, out_proj, preferred_element_type=jnp.float32)
    squares = squares[:, :, 0].T.reshape(-1)
    summed, square_own = scattered(partial_value.astype(jnp.bfloat16), squares)
    mixed = (summed * lax.rsqrt(square_own / out_gain.shape[0] + EPSILON)[:, None]).astype(jnp.bfloat16)
    return (mixed, base_state)


def solution(mesh):
    placed = (
        P(("dp", "kv", "tp"), None),
        P(),
        P(None, ("kv", "tp")),
        P(None, ("kv", "tp")),
        P(None, ("kv", "tp")),
        P(None, ("kv", "tp")),
        P(),
        P(),
        P(),
        P(),
        P(),
        P(),
        P(),
        P(),
        P(("kv", "tp"), None),
        P("dp", ("kv", "tp"), None, None),
        P("dp", None, ("kv", "tp")),
        P("dp", None, ("kv", "tp")),
        P("dp", None, ("kv", "tp")),
        P("dp", None, ("kv", "tp")),
        P("dp"),
    )
    return jax.shard_map(
        body,
        mesh=mesh,
        in_specs=placed,
        out_specs=(P(("dp", "kv", "tp"), None), P("dp", ("kv", "tp"), None, None)),
        check_vma=False,
    )
```

profile of v0, /device:TPU:0, one launch (start us, length us, event | category | flops | bytes accessed | tf_op | source)
XLA Modules:
  0.0 70.3 jit_solution(4608328074448717437)
XLA Ops:
  0.6 0.0 copy-start
  0.7 0.1 pad_add_fusion.rank_ref
  0.7 1.2 %fusion.26 = f32[32]{0:T(128)S(1)} fusion(bf16[32,2048]{1,0:T(8,128)(2,1)} %param.21), kind=kLoop, calls=%fused_computation.25 | loop fusion | flops 196576 | bytes 131200 | tf_op jit(solution)/shard_map/reduce_sum | solution.py:552
  1.9 0.7 %pad_maximum_fusion = f32[3,64]{1,0:T(4,128)S(1)} fusion(f32[1,64]{1,0:T(1,128)} %bitcast.51, f32[1,64]{1,0:T(1,128)} %bitcast.52, f32[1,64]{1,0:T(1,128)} %bitcast.53), kind=kLoop, calls=%fused_computation.39 | loop fusion | flops 384 | bytes 1536 | tf_op jit(solution)/shard_map/stack | solution.py:572
  2.6 0.1 constant_dynamic-slice_fusion.par_ref
  2.7 0.8 %constant_dynamic-slice_fusion.1 = bf16[2048,8]{0,1:T(8,128)(2,1)S(1)} fusion(bf16[2048,64]{0,1:T(8,128)(2,1)} %param.27, s32[]{:T(128)S(6)} %select_n.17), kind=kLoop, calls=%fused_computation.44 | loop fusion | bytes 65540 | tf_op jit(solution)/shard_map/dynamic_slice | solution.py:568
  3.5 0.7 %copy.31.acc_ref = s32[64,1]{1,0:T(8,128)S(1)} copy(s32[64,1]{0,1:T(1,128)} %bitcast.50) | data formatting | bytes 512 | tf_op jit(solution)/shard_map/broadcast_in_dim | solution.py:607
  4.2 1.0 %fusion.28.own_ref = bf16[32,2048]{1,0:T(8,128)(2,1)S(1)} fusion(bf16[32,2048]{1,0:T(8,128)(2,1)} %param.21, f32[2048]{0:T(1024)} %param.22, f32[32]{0:T(128)S(1)} %add_rsqrt_fusion.1), kind=kLoop, calls=%fused_computation.27 | loop fusion | flops 262144 | bytes 270464 | tf_op jit(solution)/shard_map/convert_element_type | solution.py:554
  5.2 0.8 %copy.30 = f32[64,4,8]{2,0,1:T(8,128)S(1)} copy(f32[64,4,8]{0,2,1:T(8,128)} %param.40) | data formatting | bytes 16384 | tf_op args[19]
  6.0 1.0 %copy.35 = bf16[2048,8]{1,0:T(8,128)(2,1)} copy(bf16[2048,8]{0,1:T(8,128)(2,1)S(1)} %constant_dynamic-slice_fusion.1) | data formatting | bytes 65536
  7.0 16.3 %gather.1 = bf16[4,2,32,2048]{3,2,1,0:T(8,128)(2,1)S(1)} custom-call(bf16[32,2048]{1,0:T(8,128)(2,1)S(1)} %fusion.28.own_ref), custom_call_target="tpu_custom_call" | custom-call | tf_op jit(solution)/shard_map/gather/pallas_call | solution.py:351
  23.4 1.2 %reshape_reshape.6 = bf16[64,4,2048]{2,1,0:T(4,128)(2,1)} reshape(bf16[4,2,32,2048]{3,2,1,0:T(8,128)(2,1)S(1)} %gather.1) | data formatting | bytes 2097152 | tf_op jit(solution)/shard_map/reshape;reshape | solution.py:556
  24.6 2.8 %fusion.7.steps_ref.write_ref.read_ref = f32[4,64,384]{2,1,0:T(8,128)S(1)} fusion(bf16[2048,8]{1,0:T(8,128)(2,1)} %copy.35, bf16[2048,128]{1,0:T(8,128)(2,1)} %param.26, bf16[2048,128]{1,0:T(8,128)(2,1)} %param.25, bf16[64,4,2048]{2,1,0:T(4,128)(2,1)} %reshape_reshape.6), kind=kOutput, calls=%fused_computation.9 | convolution fusion | flops 408944640 | bytes 2523136 | tf_op jit(solution)/shard_map/dot_general | solution.py:560
  27.4 0.0 copy-start.10
  27.4 0.9 %fusion.16.inner_ref = bf16[4,64,512]{2,1,0:T(8,128)(2,1)S(1)} fusion(bf16[2048,512]{1,0:T(8,128)(2,1)S(1)} %copy-done.9, bf16[64,4,2048]{2,1,0:T(4,128)(2,1)S(1)} %copy-done.8), kind=kOutput, calls=%fused_computation.15 | convolution fusion | flops 537001984 | bytes 3407872 | tf_op jit(solution)/shard_map/dot_general | solution.py:560
  28.3 0.7 copy-done.10
  29.0 0.0 copy-start.5
  29.0 0.0 copy-start.6
  29.0 0.0 copy-start.7
  29.0 0.9 %fusion.13.gate_ref = bf16[4,64,512]{2,1,0:T(8,128)(2,1)S(1)} fusion(bf16[2048,512]{1,0:T(8,128)(2,1)S(1)} %copy-done.10, bf16[64,4,2048]{2,1,0:T(4,128)(2,1)S(1)} %copy-done.8), kind=kOutput, calls=%fused_computation.14 | convolution fusion | flops 537001984 | bytes 3407872 | tf_op jit(solution)/shard_map/dot_general | solution.py:560
  30.0 0.1 copy-done.1
  30.0 0.0 copy-done.2
  30.0 0.1 copy-done.3
  30.1 22.1 %mix.1 = (bf16[4,64,512]{2,1,0:T(8,128)(2,1)S(1)}, f32[4,64,128]{2,1,0:T(8,128)S(1)}, f32[64,512,128]{2,1,0:T(8,128)}) custom-call(s32[2]{0:T(128)S(1)} %pad_add_fusion.rank_ref, s32[64,1]{1,0:T(8,128)S(1)} %copy.31.acc_ref, f32[4,64,384]{2,1,0:T(8,128)S(1)} %fusion.7.steps_ref.write_ref.read_ref, f32[4,64,8]{2,1,0:T(8,128)S(1)} %bitcast.41, ...), custom_call_target="tpu_custom_call" | custom-call | tf_op jit(solution)/shard_map/mix/pallas_call | solution.py:186
  52.2 0.2 copy.32
  52.4 0.1 reshape.78
  52.5 0.1 slice_reduce_fusion
  52.6 0.1 copy.33
  52.7 0.1 reshape_reshape.7
  52.8 0.7 %convolution_convert_fusion = bf16[256,2048]{1,0:T(8,128)(2,1)S(1)} fusion(bf16[256,512]{1,0:T(8,128)(2,1)S(1)} %reshape.78, bf16[512,2048]{1,0:T(8,128)(2,1)S(1)} %copy-done), kind=kOutput, calls=%fused_computation.2 | convolution fusion | flops 537395200 | bytes 3407872 | tf_op jit(solution)/shard_map/dot_general | solution.py:624
  53.5 15.9 %scatter.1 = (f32[32,2048]{1,0:T(8,128)S(1)}, f32[8,8,128]{2,1,0:T(8,128)S(1)}) custom-call(bf16[4,2,32,2048]{3,2,1,0:T(8,128)(2,1)S(1)} %bitcast.40, f32[8,8,128]{2,1,0:T(8,128)S(1)} %pad.9.sq), custom_call_target="tpu_custom_call" | custom-call | tf_op jit(solution)/shard_map/scatter/pallas_call | solution.py:499
  69.5 0.7 %multiply_convert_fusion = bf16[32,2048]{1,0:T(8,128)(2,1)} fusion(f32[32,2048]{1,0:T(8,128)S(1)} %get-tuple-element.9, f32[32]{0:T(128)S(1)} %add_rsqrt_fusion), kind=kLoop, calls=%fused_computation.28 | loop fusion | flops 131072 | bytes 393344 | tf_op jit(solution)/shard_map/convert_element_type | solution.py:627
  (19 shorter events, 0.1 us)
Async XLA Ops:
  0.6 52.2 %copy-start = (bf16[512,2048]{1,0:T(8,128)(2,1)S(1)}, bf16[512,2048]{1,0:T(8,128)(2,1)}, u32[]{:S(2)}) copy-start(bf16[512,2048]{1,0:T(8,128)(2,1)} %param.35) | copy-start | bytes 6291460
  24.6 2.8 %copy-start.8 = (bf16[64,4,2048]{2,1,0:T(4,128)(2,1)S(1)}, bf16[64,4,2048]{2,1,0:T(4,128)(2,1)}, u32[]{:S(2)}) copy-start(bf16[64,4,2048]{2,1,0:T(4,128)(2,1)} %reshape_reshape.6) | copy-start | bytes 3145732
  24.6 2.8 %copy-start.9 = (bf16[2048,512]{1,0:T(8,128)(2,1)S(1)}, bf16[2048,512]{1,0:T(8,128)(2,1)}, u32[]{:S(2)}) copy-start(bf16[2048,512]{1,0:T(8,128)(2,1)} %param.24) | copy-start | bytes 6291460
  27.4 1.6 %copy-start.10 = (bf16[2048,512]{1,0:T(8,128)(2,1)S(1)}, bf16[2048,512]{1,0:T(8,128)(2,1)}, u32[]{:S(2)}) copy-start(bf16[2048,512]{1,0:T(8,128)(2,1)} %param.23) | copy-start | bytes 6291460
  29.0 1.0 %copy-start.1 = (bf16[64,7,512]{2,0,1:T(8,128)(2,1)S(1)}, bf16[64,7,512]{2,0,1:T(8,128)(2,1)}, u32[]{:S(2)}) copy-start(bf16[64,7,512]{2,0,1:T(8,128)(2,1)} %param.37) | copy-start | bytes 1376260
  29.0 1.0 %copy-start.2 = (bf16[64,7,128]{2,0,1:T(8,128)(2,1)S(1)}, bf16[64,7,128]{2,0,1:T(8,128)(2,1)}, u32[]{:S(2)}) copy-start(bf16[64,7,128]{2,0,1:T(8,128)(2,1)} %param.38) | copy-start | bytes 344068
  29.0 1.1 %copy-start.3 = (bf16[64,7,128]{2,0,1:T(8,128)(2,1)S(1)}, bf16[64,7,128]{2,0,1:T(8,128)(2,1)}, u32[]{:S(2)}) copy-start(bf16[64,7,128]{2,0,1:T(8,128)(2,1)} %param.39) | copy-start | bytes 344068
  29.0 1.1 %copy-start.4 = (bf16[4,4096]{1,0:T(4,128)(2,1)S(1)}, bf16[4,4096]{1,0:T(4,128)(2,1)}, u32[]{:S(2)}) copy-start(bf16[4,4096]{1,0:T(4,128)(2,1)} %taps_inner_ref.1) | copy-start | bytes 98308
  29.0 1.1 %copy-start.5 = (f32[4096]{0:T(1024)S(1)}, f32[4096]{0:T(1024)}, u32[]{:S(2)}) copy-start(f32[4096]{0:T(1024)} %param.34) | copy-start | bytes 49156
  29.0 1.1 %copy-start.6 = (bf16[4,1024]{1,0:T(4,128)(2,1)S(1)}, bf16[4,1024]{1,0:T(4,128)(2,1)}, u32[]{:S(2)}) copy-start(bf16[4,1024]{1,0:T(4,128)(2,1)} %taps_write_ref.1) | copy-start | bytes 24580
  29.0 1.1 %copy-start.7 = (bf16[4,1024]{1,0:T(4,128)(2,1)S(1)}, bf16[4,1024]{1,0:T(4,128)(2,1)}, u32[]{:S(2)}) copy-start(bf16[4,1024]{1,0:T(4,128)(2,1)} %taps_read_ref.1) | copy-start | bytes 24580
where the time goes:
time: 70.8 us; the launch traced here: 70.3 us
  Pallas kernels  54.4 us (77%)
  local copies, waits for them, and re-layouts  6.02 us (9%)
  matrix products  5.32 us (8%)
  other arithmetic  3.76 us (5%)
  between operations  0.79 us (1%)
    pallas_call x1, Pallas kernels, mix(): pl.pallas_call(mix_kernel, grid_spec=pltpu.PrefetchScalarGridSpec(num_sca...  22.1 us
    pallas_call x1, Pallas kernels, gathered(): pl.pallas_call(functools.partial(gather_kernel, n), out_shape=jax.ShapeDt...  16.3 us
    pallas_call x1, Pallas kernels, scattered(): pl.pallas_call(functools.partial(scatter_kernel, n), out_shape=[jax.Shape...  15.9 us
    dot_general x3, matrix products, project(): out = jnp.dot(normed, weight, preferred_element_type=jnp.float32)  4.6 us
    unnamed x24, local copies, waits for them, and re-layouts  2.66 us

commit v1 on v0

--- a/solution.py
+++ b/solution.py
@@ -515,6 +515,811 @@
     return summed, jnp.sum(sqs[:, 0, :rows], axis=0)
 
 
+def pick(x, rows, first):
+    wide = jnp.broadcast_to(x, (rows, x.shape[1]))
+    lane = lax.broadcasted_iota(jnp.int32, wide.shape, 1)
+    row = lax.broadcasted_iota(jnp.int32, wide.shape, 0)
+    return jnp.sum(jnp.where(lane == row + first, wide, 0.0), axis=1, keepdims=True)
+
+
+def turn_rows(rows, props, back=False):
+    seqs = rows // props
+    row = lax.broadcasted_iota(jnp.int32, (rows, rows), 0)
+    col = lax.broadcasted_iota(jnp.int32, (rows, rows), 1)
+    if back:
+        row, col = col, row
+    return jnp.where(col == row % seqs * props + row // seqs, 1.0, 0.0).astype(jnp.bfloat16)
+
+
+def silu_of(x):
+    return x / (1.0 + jnp.exp(-x))
+
+
+def round_of(x):
+    return x.astype(jnp.bfloat16).astype(jnp.float32)
+
+
+def split_of(x):
+    high = x.astype(jnp.bfloat16)
+    return high, (x - high.astype(jnp.float32)).astype(jnp.bfloat16)
+
+
+def own_slice(ref, first, count):
+    return ref[:, pl.ds(pl.multiple_of(first, 128), count)].astype(jnp.float32)
+
+
+def lead_kernel(
+    n,
+    tokens_hbm,
+    norm_hbm,
+    acc_hbm,
+    last_hbm,
+    decay_hbm,
+    hist_inner_hbm,
+    hist_write_hbm,
+    hist_read_hbm,
+    taps_inner_hbm,
+    taps_write_hbm,
+    taps_read_hbm,
+    state_ref,
+    rows_ref,
+    base_ref,
+    half_ref,
+    part_inner_ref,
+    part_write_ref,
+    part_read_ref,
+    own_ref,
+    decay_buf,
+    wide_buf,
+    turned_buf,
+    old_buf,
+    rs,
+    rr,
+    ls,
+    lr,
+    fs,
+    fr,
+    local_sem,
+    state_sems,
+    small_sems,
+    tokens_ref,
+    norm_ref,
+    acc_ref,
+    last_ref,
+    decay_ref,
+    hist_inner_ref,
+    hist_write_ref,
+    hist_read_ref,
+    taps_inner_ref,
+    taps_write_ref,
+    taps_read_ref,
+):
+    f32 = jnp.float32
+    bf16 = jnp.bfloat16
+    k = lax.axis_index("kv")
+    t = lax.axis_index("tp")
+    rank = k * 2 + t
+    right = {"kv": lax.rem(k + 1, n)}
+    left = {"kv": lax.rem(k + n - 1, n)}
+    partner = {"tp": 1 - t}
+    barrier = pltpu.get_barrier_semaphore()
+    pl.semaphore_signal(barrier, inc=1, device_id=partner, device_id_type=MESH)
+
+    @pl.when(k < n - 1)
+    def _():
+        pl.semaphore_signal(barrier, inc=1, device_id=right, device_id_type=MESH)
+
+    @pl.when(k > 0)
+    def _():
+        pl.semaphore_signal(barrier, inc=1, device_id=left, device_id_type=MESH)
+
+    props, heads, seqs = last_ref.shape
+    cols = base_ref.shape[1]
+    states = base_ref.shape[2]
+    hist = hist_inner_ref.shape[0]
+    width = taps_inner_ref.shape[0]
+    blocks = seqs // BLOCK
+
+    def fetch(b):
+        span = pl.ds(b * BLOCK, BLOCK)
+        return pltpu.make_async_copy(state_ref.at[span], base_ref.at[span], state_sems.at[b])
+
+    small = [
+        pltpu.make_async_copy(src, dst, small_sems.at[i])
+        for i, (src, dst) in enumerate(
+            [
+                (tokens_hbm, tokens_ref),
+                (norm_hbm, norm_ref),
+                (acc_hbm, acc_ref),
+                (last_hbm, last_ref),
+                (decay_hbm, decay_ref),
+                (hist_inner_hbm, hist_inner_ref),
+                (hist_write_hbm, hist_write_ref),
+                (hist_read_hbm, hist_read_ref),
+                (taps_inner_hbm, taps_inner_ref),
+                (taps_write_hbm, taps_write_ref),
+                (taps_read_hbm, taps_read_ref),
+            ]
+        )
+    ]
+    for c in small:
+        c.start()
+    for b in range(blocks):
+        fetch(b).start()
+    for c in small[:2]:
+        c.wait()
+    own = tokens_ref[...].astype(f32)
+    scale = lax.rsqrt(jnp.mean(own * own, axis=-1, keepdims=True) + EPSILON)
+    normed = (own * scale * norm_ref[...]).astype(bf16)
+    own_ref[...] = jnp.dot(
+        turn_rows(own.shape[0], props), normed, preferred_element_type=f32
+    ).astype(bf16)
+
+    inside = (k > 0) & (k < n - 1)
+
+    @pl.when(inside)
+    def _():
+        pl.semaphore_wait(barrier, 3)
+
+    @pl.when(jnp.logical_not(inside))
+    def _():
+        pl.semaphore_wait(barrier, 2)
+
+    span = own_ref.shape[1] // CHUNKS
+
+    def view(j, c):
+        return rows_ref.at[j, t, :, pl.ds(c * span, span)]
+
+    def mine(c):
+        return own_ref.at[:, pl.ds(c * span, span)]
+
+    def to_right(s, c):
+        j = jnp.maximum(k - s, 0)
+        return remote(mine(c) if s == 0 else view(j, c), view(j, c), rs.at[s, c], rr.at[s, c], right)
+
+    def to_left(s, c):
+        j = jnp.minimum(k + s, n - 1)
+        return remote(mine(c) if s == 0 else view(j, c), view(j, c), ls.at[s, c], lr.at[s, c], left)
+
+    def across(j, c, first=False):
+        return remote(mine(c) if first else view(j, c), view(j, c), fs.at[j, c], fr.at[j, c], partner)
+
+    def hop(s, c):
+        if s > 0:
+            @pl.when(k - s >= 0)
+            def _():
+                to_right(s - 1, c).wait_recv()
+
+            @pl.when(k + s < n)
+            def _():
+                to_left(s - 1, c).wait_recv()
+
+        if s < n - 1:
+            @pl.when((k - s >= 0) & (k < n - 1))
+            def _():
+                to_right(s, c).start()
+
+            @pl.when((k + s < n) & (k > 0))
+            def _():
+                to_left(s, c).start()
+
+        if s == 0:
+            across(k, c, True).start()
+        else:
+            @pl.when(k - s >= 0)
+            def _():
+                across(k - s, c).start()
+
+            @pl.when(k + s < n)
+            def _():
+                across(k + s, c).start()
+
+    for c in range(CHUNKS):
+        hop(0, c)
+    local = pltpu.make_async_copy(own_ref, rows_ref.at[k, t], local_sem)
+    local.start()
+
+    for c in small[2:]:
+        c.wait()
+
+    acc_row = acc_ref[...]
+    rate = pick(-jnp.exp(decay_ref[...]), heads, rank * heads)
+    old_weights = [None] * props
+    tail = jnp.zeros((heads, seqs), f32)
+    for p in reversed(range(props)):
+        mask = jnp.where(acc_row > p, 1.0, 0.0)
+        old_weights[p] = mask * jnp.exp(tail) * last_ref[p]
+        tail = tail + rate * last_ref[p] * mask
+    turned = jnp.transpose(jnp.concatenate(old_weights + [jnp.exp(tail)], axis=0))
+    lane = lax.broadcasted_iota(jnp.int32, (heads, cols), 1)
+    row = lax.broadcasted_iota(jnp.int32, (heads, cols), 0)
+    expand = jnp.where(lane // (cols // heads) == row, 1.0, 0.0).astype(bf16)
+    for p in range(props):
+        w = turned[:, p * heads : (p + 1) * heads]
+        high, low = split_of(w)
+        wide_buf[p] = jnp.dot(high, expand, preferred_element_type=f32) + jnp.dot(
+            low, expand, preferred_element_type=f32
+        )
+    for h in range(heads):
+        at = props * heads + h
+        decay_buf[h] = jnp.broadcast_to(turned[:, at : at + 1], (seqs, states))
+    acc = jnp.sum(
+        jnp.where(
+            lax.broadcasted_iota(jnp.int32, (seqs, seqs), 0)
+            == lax.broadcasted_iota(jnp.int32, (seqs, seqs), 1),
+            jnp.broadcast_to(acc_row, (seqs, seqs)),
+            0,
+        ).astype(f32),
+        axis=1,
+        keepdims=True,
+    )
+
+    def conv_parts(hist_at, taps, part_ref, b):
+        where_at = jnp.broadcast_to(acc[b : b + BLOCK], hist_at[0].shape)
+        current = []
+        for e in range(width - 1):
+            r = hist_at[e]
+            for v in range(1, hist - width + 2):
+                r = jnp.where(where_at == v, hist_at[e + v], r)
+            current.append(r)
+        for i in range(width - 1):
+            total = taps[0:1] * current[i]
+            for e in range(i + 1, width - 1):
+                total = total + taps[e - i : e - i + 1] * current[e]
+            part_ref[i, b : b + BLOCK, :] = total
+
+    def conv_old(hist_at, taps):
+        res = []
+        for r in range(hist - width + 1):
+            total = taps[0:1] * hist_at[r]
+            for e in range(1, width):
+                total = total + taps[e : e + 1] * hist_at[r + e]
+            res.append(silu_of(total))
+        return res
+
+    def slabs(ref, b):
+        return [ref[e, b : b + BLOCK, :].astype(f32) for e in range(hist)]
+
+    taps_inner = own_slice(taps_inner_ref, rank * cols, cols)
+    taps_write = own_slice(taps_write_ref, rank * states, states)
+    taps_read = own_slice(taps_read_ref, rank * states, states)
+    per_half = blocks // 2
+
+    def prepare(part):
+        lefts, rights = [], []
+        for g in range(per_half):
+            b = (part * per_half + g) * BLOCK
+            h_inner = slabs(hist_inner_ref, b)
+            h_write = slabs(hist_write_ref, b)
+            olds = conv_old(h_inner, taps_inner)
+            lefts += [wide_buf[p, b : b + BLOCK, :] * olds[p] for p in range(props)]
+            rights += conv_old(h_write, taps_write)
+            conv_parts(h_inner, taps_inner, part_inner_ref, b)
+            conv_parts(h_write, taps_write, part_write_ref, b)
+            conv_parts(slabs(hist_read_ref, b), taps_read, part_read_ref, b)
+        turned_buf[part] = jnp.transpose(jnp.concatenate(lefts, axis=0)).astype(bf16)
+        old_buf[part] = jnp.concatenate(rights, axis=0).astype(bf16)
+
+    half_rows = per_half * props * BLOCK
+    row = lax.broadcasted_iota(jnp.int32, (half_rows, states), 0)
+    seq_of = row // (props * BLOCK) * BLOCK + row % BLOCK
+
+    def update(part, first, count):
+        lhs = turned_buf[part]
+        old = old_buf[part].astype(f32)
+        head_dim = cols // heads
+
+        def pair(i, carry):
+            at = first + 2 * i
+            rhs = jnp.concatenate(
+                [jnp.where(seq_of == at + e, old, 0.0).astype(bf16) for e in range(2)], axis=1
+            )
+            add = jnp.dot(lhs, rhs, preferred_element_type=f32)
+            for e in range(2):
+                s = part * (seqs // 2) + at + e
+                for h in range(heads):
+                    lo, hi = h * head_dim, (h + 1) * head_dim
+                    d = decay_buf[h, pl.ds(s, 1), :]
+                    new = d * base_ref[s, lo:hi, :] + add[lo:hi, e * states : (e + 1) * states]
+                    base_ref[s, lo:hi, :] = new
+                    half_ref[s, lo:hi, :] = new.astype(bf16)
+            return carry
+
+        lax.fori_loop(0, count // 2, pair, 0)
+
+    hops = [(s, c) for s in range(1, n) for c in range(CHUNKS)]
+    done = 0
+    for part in range(2):
+        prepare(part)
+        for g in range(per_half):
+            b = part * per_half + g
+            fetch(b).wait()
+            update(part, g * BLOCK, BLOCK)
+            goal = len(hops) * (b + 1) // blocks
+            while done < goal:
+                hop(*hops[done])
+                done += 1
+    local.wait()
+    for s in range(n - 1):
+        for c in range(CHUNKS):
+            @pl.when((k - s >= 0) & (k < n - 1))
+            def _():
+                to_right(s, c).wait_send()
+
+            @pl.when((k + s < n) & (k > 0))
+            def _():
+                to_left(s, c).wait_send()
+    for j in range(n):
+        for c in range(CHUNKS):
+            across(j, c).wait_send()
+            there = rows_ref.at[j, 1 - t, :, pl.ds(c * span, span)]
+            remote(there, there, fs.at[j, c], fr.at[j, c], partner).wait_recv()
+
+
+kept = pltpu.with_memory_space_constraint
+
+
+def lead(tokens, norm_gain, acc, last, decay_log, hi, hw, hr, ci, cw, cr, state):
+    n = lax.axis_size("kv")
+    rows, width = tokens.shape
+    props, heads, seqs = last.shape
+    cols, states = state.shape[1:]
+    taps = ci.shape[0]
+    dma = pltpu.SemaphoreType.DMA
+    vmem = pl.BlockSpec(memory_space=pltpu.VMEM)
+    hbm = pl.BlockSpec(memory_space=pltpu.HBM)
+    f32, bf16 = jnp.float32, jnp.bfloat16
+    shape = jax.ShapeDtypeStruct
+    blocks = seqs // BLOCK
+    half_rows = seqs // 2 * props
+    small = (tokens, norm_gain, acc, last, decay_log, hi, hw, hr, ci, cw, cr)
+    return pl.pallas_call(
+        functools.partial(lead_kernel, n),
+        out_shape=[
+            shape((n, 2, rows, width), bf16),
+            pltpu.VMEM(state.shape, f32),
+            pltpu.VMEM(state.shape, bf16),
+            shape((taps - 1, seqs, cols), f32),
+            shape((taps - 1, seqs, states), f32),
+            shape((taps - 1, seqs, states), f32),
+        ],
+        in_specs=[hbm] * (len(small) + 1),
+        out_specs=[vmem] * 6,
+        scratch_shapes=[
+            pltpu.VMEM((rows, width), bf16),
+            pltpu.VMEM((heads, seqs, states), f32),
+            pltpu.VMEM((props, seqs, cols), f32),
+            pltpu.VMEM((2, cols, half_rows), bf16),
+            pltpu.VMEM((2, half_rows, states), bf16),
+        ]
+        + [dma((n - 1, CHUNKS))] * 4
+        + [dma((n, CHUNKS))] * 2
+        + [dma, dma((blocks,)), dma((len(small),))]
+        + [pltpu.VMEM(x.shape, x.dtype) for x in small],
+        compiler_params=pltpu.CompilerParams(
+            collective_id=2, has_side_effects=True, vmem_limit_bytes=8 * 1024 * 1024
+        ),
+        name="lead",
+    )(*[kept(x, pltpu.HBM) for x in small + (state,)])
+
+
+def core_kernel(
+    heads,
+    rank_ref,
+    rows_ref,
+    base_ref,
+    half_ref,
+    part_inner_ref,
+    part_write_ref,
+    part_read_ref,
+    inner_ref,
+    write_ref,
+    read_ref,
+    step_ref,
+    gate_ref,
+    outw_ref,
+    bias_ref,
+    decay_ref,
+    skip_ref,
+    taps_inner_ref,
+    taps_write_ref,
+    taps_read_ref,
+    gain_ref,
+    out_ref,
+    sq_ref,
+    state_out,
+    gate_buf,
+    inner_buf,
+    write_buf,
+    read_buf,
+    step_buf,
+    un_buf,
+    sems,
+):
+    f32, bf16 = jnp.float32, jnp.bfloat16
+    rank = rank_ref[0]
+    seqs, cols, states = base_ref.shape
+    blocks = seqs // BLOCK
+    props = rows_ref.shape[0] // seqs
+    width = taps_inner_ref.shape[0]
+    head_count = step_ref.shape[0]
+
+    def flush(b):
+        span = pl.ds(b * BLOCK, BLOCK)
+        return pltpu.make_async_copy(base_ref.at[span], state_out.at[span], sems.at[b])
+
+    for b in range(blocks):
+        flush(b).start()
+    rows = rows_ref[...]
+    tile = 256
+    for w_ref, buf in ((inner_ref, inner_buf), (gate_ref, gate_buf)):
+        for lo in range(0, cols, tile):
+            buf[:, lo : lo + tile] = round_of(
+                jnp.dot(rows, w_ref[:, lo : lo + tile], preferred_element_type=f32)
+            )
+    both = jnp.dot(
+        rows, jnp.concatenate([write_ref[...], read_ref[...]], axis=1), preferred_element_type=f32
+    )
+    write_buf[...] = round_of(both[:, :states])
+    read_buf[...] = round_of(both[:, states:])
+    nt = (((1,), (1,)), ((), ()))
+    step_buf[...] = lax.dot_general(rows, step_ref[...], nt, preferred_element_type=f32)
+    taps_inner = own_slice(taps_inner_ref, rank * cols, cols)
+    taps_write = own_slice(taps_write_ref, rank * states, states)
+    taps_read = own_slice(taps_read_ref, rank * states, states)
+    gain = own_slice(gain_ref, rank * cols, cols)
+    bias = bias_ref[...]
+    rate = -jnp.exp(decay_ref[...])
+    skip = skip_ref[...]
+    lane = lax.broadcasted_iota(jnp.int32, (2 * head_count, cols), 1)
+    row = lax.broadcasted_iota(jnp.int32, (2 * head_count, cols), 0)
+    expand = jnp.where(
+        lane // (cols // heads) + rank * heads == row % head_count, 1.0, 0.0
+    ).astype(bf16)
+    lane_of = lax.broadcasted_iota(jnp.int32, (BLOCK, 128), 1)
+    row_r = lax.broadcasted_iota(jnp.int32, (props * BLOCK, states), 0) % BLOCK
+
+    def block(r, carry):
+        at_row = pl.multiple_of(r * props * BLOCK, props * BLOCK)
+        at_seq = pl.multiple_of(r * BLOCK, BLOCK)
+
+        def news(buf, part_ref, taps):
+            fresh = [buf[pl.ds(at_row + i * BLOCK, BLOCK), :] for i in range(props)]
+            res = []
+            for i in range(props):
+                total = taps[width - 1 : width] * fresh[i]
+                for e in range(1, min(i, width - 1) + 1):
+                    total = total + taps[width - 1 - e : width - e] * fresh[i - e]
+                if i < width - 1:
+                    total = total + part_ref[i, pl.ds(at_seq, BLOCK), :]
+                res.append(silu_of(total))
+            return res
+
+        inner_new = news(inner_buf, part_inner_ref, taps_inner)
+        write_new = [round_of(x) for x in news(write_buf, part_write_ref, taps_write)]
+        read_new = [round_of(x) for x in news(read_buf, part_read_ref, taps_read)]
+        steps = step_buf[pl.ds(at_row, props * BLOCK), :] + bias
+        steps = jnp.maximum(steps, 0.0) + jnp.log1p(jnp.exp(-jnp.abs(steps)))
+        step = [steps[i * BLOCK : (i + 1) * BLOCK] for i in range(props)]
+        cums = []
+        for i in range(props):
+            cums.append(rate * step[i] + (cums[-1] if cums else 0.0))
+        coefs = []
+        where_of = {}
+        for i in range(props):
+            for j in range(i + 1):
+                score = jnp.sum(read_new[i] * write_new[j], axis=-1, keepdims=True)
+                c = jnp.exp(cums[i] - cums[j]) * step[j] * score
+                if i == j:
+                    c = c + skip
+                where_of[(i, j)] = len(coefs)
+                coefs.append(c)
+        first_cum = len(coefs)
+        coefs += [jnp.exp(c) for c in cums]
+        high, low = split_of(jnp.concatenate(coefs, axis=0))
+        wide = jnp.dot(
+            jnp.concatenate([high, low], axis=1), expand, preferred_element_type=f32
+        )
+
+        def at(e):
+            return wide[e * BLOCK : (e + 1) * BLOCK]
+
+        read_all = jnp.concatenate(read_new, axis=0)
+        carried = None
+        for s in range(0, BLOCK, 2):
+            lhs = jnp.concatenate(
+                [jnp.where(row_r == s + e, read_all, 0.0).astype(bf16) for e in range(2)], axis=1
+            )
+            rhs = jnp.concatenate([half_ref[at_seq + s + e] for e in range(2)], axis=1)
+            got = lax.dot_general(lhs, rhs, nt, preferred_element_type=f32)
+            carried = got if carried is None else carried + got
+        squares = jnp.zeros((BLOCK, 128), f32)
+        outs = []
+        for i in range(props):
+            y = at(first_cum + i) * carried[i * BLOCK : (i + 1) * BLOCK]
+            for j in range(i + 1):
+                y = y + at(where_of[(i, j)]) * inner_new[j]
+            g = y * silu_of(gate_buf[pl.ds(at_row + i * BLOCK, BLOCK), :])
+            squares = jnp.where(lane_of == i, jnp.sum(g * g, axis=-1, keepdims=True), squares)
+            outs.append(g * gain)
+        sq_ref[r] = squares
+        un_buf[pl.ds(at_row, props * BLOCK), :] = jnp.concatenate(outs, axis=0).astype(bf16)
+        return carry
+
+    lax.fori_loop(0, blocks, block, 0)
+    un = un_buf[...]
+    wide_tile = 512
+    for lo in range(0, outw_ref.shape[1], wide_tile):
+        out_ref[:, lo : lo + wide_tile] = jnp.dot(
+            un, outw_ref[:, lo : lo + wide_tile], preferred_element_type=f32
+        ).astype(bf16)
+    for b in range(blocks):
+        flush(b).wait()
+
+
+def core(rank, heads, rows, base, half, parts, weights, bias, decay_log, skip, ci, cw, cr, gain):
+    seqs, cols, states = base.shape
+    tokens = rows.shape[0]
+    width = weights[-1].shape[1]
+    ranks = seqs // BLOCK
+    f32, bf16 = jnp.float32, jnp.bfloat16
+    vmem = pl.BlockSpec(memory_space=pltpu.VMEM)
+    shape = jax.ShapeDtypeStruct
+    return pl.pallas_call(
+        functools.partial(core_kernel, heads),
+        out_shape=[
+            shape((tokens, width), bf16),
+            shape((ranks, BLOCK, 128), f32),
+            pltpu.HBM(base.shape, f32),
+        ],
+        in_specs=[pl.BlockSpec(memory_space=pltpu.SMEM)] + [vmem] * 19,
+        out_specs=[vmem, vmem, pl.BlockSpec(memory_space=pl.ANY)],
+        scratch_shapes=[
+            pltpu.VMEM((tokens, cols), f32),
+            pltpu.VMEM((tokens, cols), f32),
+            pltpu.VMEM((tokens, states), f32),
+            pltpu.VMEM((tokens, states), f32),
+            pltpu.VMEM((tokens, weights[3].shape[0]), f32),
+            pltpu.VMEM((tokens, cols), bf16),
+            pltpu.SemaphoreType.DMA((ranks,)),
+        ],
+        compiler_params=pltpu.CompilerParams(vmem_limit_bytes=8 * 1024 * 1024),
+        name="core",
+    )(rank, rows, kept(base, pltpu.VMEM), kept(half, pltpu.VMEM), *parts, *weights, bias, decay_log, skip, ci, cw, cr, gain)
+
+
+def tail_kernel(
+    n, channels, part, sq, mixed, sqs, out, turned, pbuf, rbuf, lbuf, rout, lout, ps, pr, rs, rr, ls, lr, ss, sr
+):
+    f32 = jnp.float32
+    k = lax.axis_index("kv")
+    t = lax.axis_index("tp")
+    rank = k * 2 + t
+    ranks = n * 2
+    right = {"kv": lax.rem(k + 1, n)}
+    left = {"kv": lax.rem(k + n - 1, n)}
+    partner = {"tp": 1 - t}
+    span = part.shape[3] // CHUNKS
+    barrier = pltpu.get_barrier_semaphore()
+
+    def peer(o):
+        p = lax.rem(rank + o, ranks)
+        return {"kv": p // 2, "tp": lax.rem(p, 2)}
+
+    for o in range(1, ranks):
+        pl.semaphore_signal(barrier, inc=1, device_id=peer(o), device_id_type=MESH)
+    pl.semaphore_wait(barrier, ranks - 1)
+
+    def cut(c):
+        return pl.ds(c * span, span)
+
+    def across(j, c):
+        return remote(
+            part.at[j, 1 - t, :, cut(c)], pbuf.at[j, :, cut(c)], ps.at[j, c], pr.at[j, c], partner
+        )
+
+    def to_right(d, c):
+        return remote(
+            rout.at[d, :, cut(c)], rbuf.at[d, :, cut(c)], rs.at[d, c], rr.at[d, c], right
+        )
+
+    def to_left(d, c):
+        return remote(lout.at[d, :, cut(c)], lbuf.at[d, :, cut(c)], ls.at[d, c], lr.at[d, c], left)
+
+    def square(o):
+        p = lax.rem(rank + o, ranks)
+        return remote(sq.at[p], sqs.at[rank], ss.at[o], sr.at[o], peer(o))
+
+    low = k < n // 2
+    for i in range(n):
+        j = jnp.where(low, n - 1 - i, i)
+        for c in range(CHUNKS):
+            across(j, c).start()
+    for o in range(1, ranks):
+        square(o).start()
+    sqs[rank] = sq[rank]
+
+    def pair(j, c):
+        across(j, c).wait_recv()
+        return part[j, t, :, cut(c)].astype(f32) + pbuf[j, :, cut(c)].astype(f32)
+
+    def rightward():
+        for d in range(n - 1, 0, -1):
+            for c in range(CHUNKS):
+                @pl.when((k < d) & (k == 0))
+                def _():
+                    rout[d, :, cut(c)] = pair(d, c).astype(rout.dtype)
+                    to_right(d, c).start()
+
+                @pl.when((k < d) & (k > 0))
+                def _():
+                    value = pair(d, c)
+                    to_right(d, c).wait_recv()
+                    rout[d, :, cut(c)] = (value + rbuf[d, :, cut(c)].astype(f32)).astype(rout.dtype)
+                    to_right(d, c).start()
+
+    def leftward():
+        for d in range(n - 1):
+            for c in range(CHUNKS):
+                @pl.when((k > d) & (k == n - 1))
+                def _():
+                    lout[d, :, cut(c)] = pair(d, c).astype(lout.dtype)
+                    to_left(d, c).start()
+
+                @pl.when((k > d) & (k < n - 1))
+                def _():
+                    value = pair(d, c)
+                    to_left(d, c).wait_recv()
+                    lout[d, :, cut(c)] = (value + lbuf[d, :, cut(c)].astype(f32)).astype(lout.dtype)
+                    to_left(d, c).start()
+
+    @pl.when(k < n // 2)
+    def _():
+        rightward()
+        leftward()
+
+    @pl.when(k >= n // 2)
+    def _():
+        leftward()
+        rightward()
+
+    for c in range(CHUNKS):
+        out[:, cut(c)] = pair(k, c)
+
+        @pl.when(k > 0)
+        def _():
+            to_right(k, c).wait_recv()
+            out[:, cut(c)] += rbuf[k, :, cut(c)].astype(f32)
+
+        @pl.when(k < n - 1)
+        def _():
+            to_left(k, c).wait_recv()
+            out[:, cut(c)] += lbuf[k, :, cut(c)].astype(f32)
+
+    for o in range(1, ranks):
+        square(o).wait_send()
+        source = lax.rem(rank + ranks - o, ranks)
+        remote(sq.at[rank], sqs.at[source], ss.at[o], sr.at[o], peer(o)).wait_recv()
+    scale = lax.rsqrt(jnp.sum(sqs[...], axis=0) / channels + EPSILON)
+    props = out.shape[0] // BLOCK
+    for i in range(props):
+        rows = out[i * BLOCK : (i + 1) * BLOCK, :] * scale[:, i : i + 1]
+        turned[i * BLOCK : (i + 1) * BLOCK, :] = rows
+    mixed[...] = jnp.dot(
+        turn_rows(out.shape[0], props, True),
+        turned[...].astype(mixed.dtype),
+        preferred_element_type=f32,
+    ).astype(mixed.dtype)
+    for j in range(n):
+        for c in range(CHUNKS):
+            across(j, c).wait_send()
+
+            @pl.when(k < j)
+            def _():
+                to_right(j, c).wait_send()
+
+            @pl.when(k > j)
+            def _():
+                to_left(j, c).wait_send()
+
+
+def finish(partial_value, squares, channels):
+    n = lax.axis_size("kv")
+    ranks = n * 2
+    rows = partial_value.shape[0] // ranks
+    cols = partial_value.shape[1]
+    dma = pltpu.SemaphoreType.DMA
+    vmem = pl.BlockSpec(memory_space=pltpu.VMEM)
+    kind = partial_value.dtype
+    f32 = jnp.float32
+    return pl.pallas_call(
+        functools.partial(tail_kernel, n, channels),
+        out_shape=jax.ShapeDtypeStruct((rows, cols), kind),
+        in_specs=[vmem, vmem],
+        out_specs=vmem,
+        scratch_shapes=[
+            pltpu.VMEM(squares.shape, f32),
+            pltpu.VMEM((rows, cols), f32),
+            pltpu.VMEM((rows, cols), f32),
+        ]
+        + [pltpu.VMEM((n, rows, cols), kind)] * 5
+        + [dma((n, CHUNKS))] * 6
+        + [dma((ranks,))] * 2,
+        compiler_params=pltpu.CompilerParams(
+            collective_id=3, has_side_effects=True, vmem_limit_bytes=32 * 1024 * 1024
+        ),
+        name="tail",
+    )(partial_value.reshape(n, 2, rows, cols), squares)
+
+
+def whole_groups(tokens, saved_state, last_steps):
+    span = lax.axis_size("kv") * lax.axis_size("tp")
+    return span == GROUPS and tokens.shape[0] == BLOCK * last_steps.shape[1]
+
+
+def quick(
+    tokens,
+    norm_gain,
+    gate_proj,
+    inner_proj,
+    write_proj,
+    read_proj,
+    step_proj,
+    step_bias,
+    decay_log,
+    skip_gain,
+    conv_inner,
+    conv_write,
+    conv_read,
+    out_gain,
+    out_proj,
+    saved_state,
+    inner_history,
+    write_history,
+    read_history,
+    last_steps,
+    accepted,
+):
+    device_rank = lax.axis_index(("kv", "tp"))
+    seqs, heads, head_dim, states = saved_state.shape
+    slab = lambda x: x.transpose(1, 0, 2)
+    row = lambda x: x.reshape(1, -1)
+    weights = (inner_proj, write_proj, read_proj, step_proj.T, gate_proj, out_proj)
+    got = lead(
+        tokens,
+        row(norm_gain),
+        row(accepted),
+        last_steps.transpose(1, 2, 0),
+        row(decay_log),
+        slab(inner_history),
+        slab(write_history),
+        slab(read_history),
+        conv_inner,
+        conv_write,
+        conv_read,
+        saved_state.reshape(seqs, heads * head_dim, states),
+    )
+    rows, base, half = got[:3]
+    partial_value, squares, base_state = core(
+        device_rank.reshape(1).astype(jnp.int32),
+        heads,
+        rows.reshape(-1, rows.shape[-1]),
+        base,
+        half,
+        got[3:6],
+        weights,
+        row(step_bias),
+        row(decay_log),
+        row(skip_gain),
+        conv_inner,
+        conv_write,
+        conv_read,
+        row(out_gain),
+    )
+    mixed = finish(partial_value, squares, out_gain.shape[0])
+    return (mixed, base_state.reshape(saved_state.shape))
+
+
 def body(
     tokens,
     norm_gain,
@@ -538,6 +1343,30 @@
     last_steps,
     accepted,
 ):
+    if whole_groups(tokens, saved_state, last_steps):
+        return quick(
+            tokens,
+            norm_gain,
+            gate_proj,
+            inner_proj,
+            write_proj,
+            read_proj,
+            step_proj,
+            step_bias,
+            decay_log,
+            skip_gain,
+            conv_inner,
+            conv_write,
+            conv_read,
+            out_gain,
+            out_proj,
+            saved_state,
+            inner_history,
+            write_history,
+            read_history,
+            last_steps,
+            accepted,
+        )
     device_rank = lax.axis_index(("kv", "tp"))
     seq_count = saved_state.shape[0]
     local_heads = saved_state.shape[1]

time: 70.8 us -> 47.9 us (0.68)
  Pallas kernels: 54.4 us -> 46.1 us
  matrix products: 5.32 us -> 0 us
  local copies, waits for them, and re-layouts: 6.02 us -> 0.71 us
  other arithmetic: 3.76 us -> 0 us
    pallas_call x3, Pallas kernels: 54.4 us -> 46.1 us  [the longest x1 21.7 us: lead(): pl.pallas_call(functools.partial(lead_kernel, n), out_shape=[shape((n, 2,...]
    dot_general x4 -> x0, matrix products: 5.32 us -> none  [the longest x3 4.6 us: project(): out = jnp.dot(normed, weight, preferred_element_type=jnp.float32)]
    unnamed x24 -> x27, local copies, waits for them, and re-layouts: 2.66 us -> 0.71 us
    convert_element_type x3 -> x0, other arithmetic: 1.76 us -> none  [the longest x1 1 us: body(): normed_own = (own_rows * lax.rsqrt(jnp.mean(own_rows * own_rows, axis=-1,...]
    another operation x2 -> x0, local copies, waits for them, and re-layouts: 1.29 us -> none  [the longest x1 1.21 us: body(): normed = normed.reshape(seq_count, proposals, -1).transpose(1, 0, 2)]
    reduce_sum x2 -> x0, other arithmetic: 1.2 us -> none  [the longest x1 1.17 us: body(): jnp.mean(own_rows * own_rows, axis=-1, keepdims=True) + EPSILON]
    dynamic_slice x2 -> x0, local copies, waits for them, and re-layouts: 0.83 us -> none  [the longest x1 0.76 us: body(): step_local = lax.dynamic_slice_in_dim(step_proj, first_head, local_heads, 1)]
    another operation x2 -> x0, other arithmetic: 0.78 us -> none  [the longest x1 0.71 us: body(): jnp.stack([step_bias, decay_log, skip_gain])]
where the time goes in v1:
time: 47.9 us; the launch traced here: 47.7 us
  Pallas kernels  46.1 us (96%)
  between operations  0.87 us (2%)
  local copies, waits for them, and re-layouts  0.71 us (1%)
    pallas_call x1, Pallas kernels, lead(): pl.pallas_call(functools.partial(lead_kernel, n), out_shape=[shape((n, 2,...  21.7 us
    pallas_call x1, Pallas kernels, finish(): pl.pallas_call(functools.partial(tail_kernel, n, channels), out_shape=jax...  16.2 us
    pallas_call x1, Pallas kernels, core(): pl.pallas_call(functools.partial(core_kernel, heads), out_shape=[shape((t...  8.21 us

profile of v1, /device:TPU:0, one launch (start us, length us, event | category | flops | bytes accessed | tf_op | source)
XLA Modules:
  0.0 47.7 jit_solution(4342812255396563400)
XLA Ops:
  0.6 0.0 copy-start
  0.7 0.0 copy-start.1
  0.7 0.0 copy-start.2
  0.7 0.0 copy-start.3
  0.7 0.0 copy-start.4
  0.7 0.0 copy-start.5
  0.7 0.0 copy-start.6
  0.7 0.0 copy-start.7
  0.7 0.0 copy-start.8
  0.7 0.0 copy-start.9
  0.7 0.0 copy-start.10
  0.8 0.0 copy-start.11
  0.8 0.0 copy-start.12
  0.8 21.7 %lead.1 = (bf16[4,2,32,2048]{3,2,1,0:T(8,128)(2,1)S(1)}, f32[64,512,128]{2,1,0:T(8,128)S(1)}, bf16[64,512,128]{2,1,0:T(8,128)(2,1)S(1)}, f32[3,64,512]{2,1,0:T(8...) custom-call(bf16[32,2048]{1,0:T(8,128)(2,1)} %tokens_hbm.1, f32[1,2048]{1,0:T(1,128)} %bitcast.29, ...), custom_call_target="tpu_custom_call" | custom-call | tf_op jit(solution)/shard_map/lead/pallas_call | solution.py:876
  22.5 0.0 copy-done
  22.5 0.0 copy-done.1
  22.5 0.0 copy-done.2
  22.5 0.0 copy-done.3
  22.5 0.0 copy-done.4
  22.5 0.0 copy-done.5
  22.6 0.0 copy-done.6
  22.6 0.0 copy-done.7
  22.6 0.0 copy-done.8
  22.6 0.0 copy-done.9
  22.6 0.0 copy-done.10
  22.6 0.0 copy-done.11
  22.6 0.0 copy-done.12
  22.6 8.2 %core.1 = (bf16[256,2048]{1,0:T(8,128)(2,1)S(1)}, f32[8,8,128]{2,1,0:T(8,128)S(1)}, f32[64,512,128]{2,1,0:T(8,128)}) custom-call(s32[1]{0:T(128)} %bitcast.rank_ref, bf16[256,2048]{1,0:T(8,128)(2,1)S(1)} %bitcast.16, f32[64,512,128]{2,1,0:T(8,128)S(1)} %get-tuple-element.12.base_ref, bf16[64,512,128]{2,1,0:T(8,128)(2,1)S(1)} %get-tuple-element.13.half_ref, ...), custom_call_target="tpu_custom_call" | custom-call | tf_op jit(solution)/shard_map/core/pallas_call | solution.py:1068
  30.8 16.2 %tail.1 = bf16[32,2048]{1,0:T(8,128)(2,1)S(1)} custom-call(bf16[4,2,32,2048]{3,2,1,0:T(8,128)(2,1)S(1)} %bitcast.17, f32[8,8,128]{2,1,0:T(8,128)S(1)} %get-tuple-element.18.sq), custom_call_target="tpu_custom_call" | custom-call | tf_op jit(solution)/shard_map/tail/pallas_call | solution.py:1235
  47.0 0.7 %copy.24 = bf16[32,2048]{1,0:T(8,128)(2,1)} copy(bf16[32,2048]{1,0:T(8,128)(2,1)S(1)} %tail.1) | data formatting | bytes 262144
Async XLA Ops:
  0.6 21.9 %copy-start = (bf16[2048,512]{1,0:T(8,128)(2,1)S(1)}, bf16[2048,512]{1,0:T(8,128)(2,1)}, u32[]{:S(2)}) copy-start(bf16[2048,512]{1,0:T(8,128)(2,1)} %inner_ref.1) | copy-start | bytes 6291460
  0.7 21.9 %copy-start.1 = (bf16[2048,512]{1,0:T(8,128)(2,1)S(1)}, bf16[2048,512]{1,0:T(8,128)(2,1)}, u32[]{:S(2)}) copy-start(bf16[2048,512]{1,0:T(8,128)(2,1)} %gate_ref.1) | copy-start | bytes 6291460
  0.7 21.9 %copy-start.2 = (bf16[512,2048]{1,0:T(8,128)(2,1)S(1)}, bf16[512,2048]{1,0:T(8,128)(2,1)}, u32[]{:S(2)}) copy-start(bf16[512,2048]{1,0:T(8,128)(2,1)} %outw_ref.1) | copy-start | bytes 6291460
  0.7 21.9 %copy-start.3 = (bf16[2048,128]{1,0:T(8,128)(2,1)S(1)}, bf16[2048,128]{1,0:T(8,128)(2,1)}, u32[]{:S(2)}) copy-start(bf16[2048,128]{1,0:T(8,128)(2,1)} %write_ref.1) | copy-start | bytes 1572868
  0.7 21.9 %copy-start.4 = (bf16[2048,128]{1,0:T(8,128)(2,1)S(1)}, bf16[2048,128]{1,0:T(8,128)(2,1)}, u32[]{:S(2)}) copy-start(bf16[2048,128]{1,0:T(8,128)(2,1)} %read_ref.1) | copy-start | bytes 1572868
  0.7 21.9 %copy-start.5 = (bf16[2048,64]{0,1:T(8,128)(2,1)S(1)}, bf16[2048,64]{0,1:T(8,128)(2,1)}, u32[]{:S(2)}) copy-start(bf16[2048,64]{0,1:T(8,128)(2,1)} %param.27) | copy-start | bytes 786436
  0.7 21.9 %copy-start.6 = (bf16[4,4096]{1,0:T(4,128)(2,1)S(1)}, bf16[4,4096]{1,0:T(4,128)(2,1)}, u32[]{:S(2)}) copy-start(bf16[4,4096]{1,0:T(4,128)(2,1)} %taps_inner_ref.1) | copy-start | bytes 98308
  0.7 21.9 %copy-start.7 = (bf16[4,1024]{1,0:T(4,128)(2,1)S(1)}, bf16[4,1024]{1,0:T(4,128)(2,1)}, u32[]{:S(2)}) copy-start(bf16[4,1024]{1,0:T(4,128)(2,1)} %taps_write_ref.1) | copy-start | bytes 24580
  0.7 21.9 %copy-start.8 = (bf16[4,1024]{1,0:T(4,128)(2,1)S(1)}, bf16[4,1024]{1,0:T(4,128)(2,1)}, u32[]{:S(2)}) copy-start(bf16[4,1024]{1,0:T(4,128)(2,1)} %taps_read_ref.1) | copy-start | bytes 24580
  0.7 21.9 %copy-start.9 = (f32[4096]{0:T(1024)S(1)}, f32[4096]{0:T(1024)}, u32[]{:S(2)}) copy-start(f32[4096]{0:T(1024)} %param.34) | copy-start | bytes 49156
  0.7 21.9 %copy-start.10 = (f32[64]{0:T(128)S(1)}, f32[64]{0:T(128)}, u32[]{:S(2)}) copy-start(f32[64]{0:T(128)} %param.29) | copy-start | bytes 772
  0.8 21.9 %copy-start.11 = (f32[64]{0:T(128)S(1)}, f32[64]{0:T(128)}, u32[]{:S(2)}) copy-start(f32[64]{0:T(128)} %param.28) | copy-start | bytes 772
  0.8 21.9 %copy-start.12 = (f32[64]{0:T(128)S(1)}, f32[64]{0:T(128)}, u32[]{:S(2)}) copy-start(f32[64]{0:T(128)} %param.30) | copy-start | bytes 772

commit v2 on v1

--- a/solution.py
+++ b/solution.py
@@ -515,6 +515,11 @@
     return summed, jnp.sum(sqs[:, 0, :rows], axis=0)
 
 
+AHEAD = 3
+CARRY = 4
+HOPS_AT = (0, 1, 1, 2, 3, 4, 5, 6)
+
+
 def pick(x, rows, first):
     wide = jnp.broadcast_to(x, (rows, x.shape[1]))
     lane = lax.broadcasted_iota(jnp.int32, wide.shape, 1)
@@ -562,12 +567,24 @@
     taps_write_hbm,
     taps_read_hbm,
     state_ref,
+    inner_hbm,
+    write_hbm,
+    read_hbm,
+    step_hbm,
+    gate_hbm,
+    outw_hbm,
     rows_ref,
     base_ref,
     half_ref,
     part_inner_ref,
     part_write_ref,
     part_read_ref,
+    inner_ref,
+    write_ref,
+    read_ref,
+    step_ref,
+    gate_ref,
+    outw_ref,
     own_ref,
     decay_buf,
     wide_buf,
@@ -582,6 +599,7 @@
     local_sem,
     state_sems,
     small_sems,
+    weight_sems,
     tokens_ref,
     norm_ref,
     acc_ref,
@@ -644,8 +662,22 @@
     ]
     for c in small:
         c.start()
-    for b in range(blocks):
-        fetch(b).start()
+    weights = [
+        pltpu.make_async_copy(src, dst, weight_sems.at[i])
+        for i, (src, dst) in enumerate(
+            [
+                (inner_hbm, inner_ref),
+                (write_hbm, write_ref),
+                (read_hbm, read_ref),
+                (step_hbm, step_ref),
+                (gate_hbm, gate_ref),
+                (outw_hbm, outw_ref),
+            ]
+        )
+    ]
+    queue = [fetch(b) for b in range(blocks)] + weights
+    for c in queue[:AHEAD]:
+        c.start()
     for c in small[:2]:
         c.wait()
     own = tokens_ref[...].astype(f32)
@@ -809,23 +841,23 @@
         old = old_buf[part].astype(f32)
         head_dim = cols // heads
 
-        def pair(i, carry):
-            at = first + 2 * i
+        adds = []
+        for i in range(0, count, 2):
             rhs = jnp.concatenate(
-                [jnp.where(seq_of == at + e, old, 0.0).astype(bf16) for e in range(2)], axis=1
+                [jnp.where(seq_of == first + i + e, old, 0.0).astype(bf16) for e in range(2)],
+                axis=1,
             )
-            add = jnp.dot(lhs, rhs, preferred_element_type=f32)
-            for e in range(2):
-                s = part * (seqs // 2) + at + e
-                for h in range(heads):
-                    lo, hi = h * head_dim, (h + 1) * head_dim
-                    d = decay_buf[h, pl.ds(s, 1), :]
-                    new = d * base_ref[s, lo:hi, :] + add[lo:hi, e * states : (e + 1) * states]
-                    base_ref[s, lo:hi, :] = new
-                    half_ref[s, lo:hi, :] = new.astype(bf16)
-            return carry
-
-        lax.fori_loop(0, count // 2, pair, 0)
+            adds.append(jnp.dot(lhs, rhs, preferred_element_type=f32))
+        for i in range(count):
+            s = part * (seqs // 2) + first + i
+            add = adds[i // 2]
+            side = i % 2 * states
+            for h in range(heads):
+                lo, hi = h * head_dim, (h + 1) * head_dim
+                new = decay_buf[h, s : s + 1, :] * base_ref[s, lo:hi, :]
+                new = new + add[lo:hi, side : side + states]
+                base_ref[s, lo:hi, :] = new
+                half_ref[s, lo:hi, :] = new.astype(bf16)
 
     hops = [(s, c) for s in range(1, n) for c in range(CHUNKS)]
     done = 0
@@ -833,12 +865,17 @@
         prepare(part)
         for g in range(per_half):
             b = part * per_half + g
-            fetch(b).wait()
+            queue[b].wait()
+            more = queue[b + AHEAD : b + AHEAD + 1] if b + 1 < blocks else queue[b + AHEAD :]
+            for c in more:
+                c.start()
             update(part, g * BLOCK, BLOCK)
-            goal = len(hops) * (b + 1) // blocks
+            goal = len(hops) * HOPS_AT[b] // 6
             while done < goal:
                 hop(*hops[done])
                 done += 1
+    for w in weights:
+        w.wait()
     local.wait()
     for s in range(n - 1):
         for c in range(CHUNKS):
@@ -859,7 +896,7 @@
 kept = pltpu.with_memory_space_constraint
 
 
-def lead(tokens, norm_gain, acc, last, decay_log, hi, hw, hr, ci, cw, cr, state):
+def lead(tokens, norm_gain, acc, last, decay_log, hi, hw, hr, ci, cw, cr, state, weights):
     n = lax.axis_size("kv")
     rows, width = tokens.shape
     props, heads, seqs = last.shape
@@ -882,9 +919,10 @@
             shape((taps - 1, seqs, cols), f32),
             shape((taps - 1, seqs, states), f32),
             shape((taps - 1, seqs, states), f32),
-        ],
-        in_specs=[hbm] * (len(small) + 1),
-        out_specs=[vmem] * 6,
+        ]
+        + [pltpu.VMEM(w.shape, w.dtype) for w in weights],
+        in_specs=[hbm] * (len(small) + 1 + len(weights)),
+        out_specs=[vmem] * (6 + len(weights)),
         scratch_shapes=[
             pltpu.VMEM((rows, width), bf16),
             pltpu.VMEM((heads, seqs, states), f32),
@@ -894,13 +932,13 @@
         ]
         + [dma((n - 1, CHUNKS))] * 4
         + [dma((n, CHUNKS))] * 2
-        + [dma, dma((blocks,)), dma((len(small),))]
+        + [dma, dma((blocks,)), dma((len(small),)), dma((len(weights),))]
         + [pltpu.VMEM(x.shape, x.dtype) for x in small],
         compiler_params=pltpu.CompilerParams(
             collective_id=2, has_side_effects=True, vmem_limit_bytes=8 * 1024 * 1024
         ),
         name="lead",
-    )(*[kept(x, pltpu.HBM) for x in small + (state,)])
+    )(*[kept(x, pltpu.HBM) for x in small + (state,) + weights])
 
 
 def core_kernel(
@@ -934,6 +972,8 @@
     read_buf,
     step_buf,
     un_buf,
+    carried_buf,
+    wide_buf,
     sems,
 ):
     f32, bf16 = jnp.float32, jnp.bfloat16
@@ -977,10 +1017,16 @@
         lane // (cols // heads) + rank * heads == row % head_count, 1.0, 0.0
     ).astype(bf16)
     lane_of = lax.broadcasted_iota(jnp.int32, (BLOCK, 128), 1)
-    row_r = lax.broadcasted_iota(jnp.int32, (props * BLOCK, states), 0) % BLOCK
-
-    def block(r, carry):
-        at_row = pl.multiple_of(r * props * BLOCK, props * BLOCK)
+
+    rows_of = props * BLOCK
+    pairs_of = {}
+    for i in range(props):
+        for j in range(i + 1):
+            pairs_of[(i, j)] = len(pairs_of)
+    first_cum = len(pairs_of)
+
+    def prepare(r):
+        at_row = pl.multiple_of(r * rows_of, rows_of)
         at_seq = pl.multiple_of(r * BLOCK, BLOCK)
 
         def news(buf, part_ref, taps):
@@ -996,57 +1042,79 @@
             return res
 
         inner_new = news(inner_buf, part_inner_ref, taps_inner)
+        for i in range(props):
+            inner_buf[pl.ds(at_row + i * BLOCK, BLOCK), :] = inner_new[i]
         write_new = [round_of(x) for x in news(write_buf, part_write_ref, taps_write)]
         read_new = [round_of(x) for x in news(read_buf, part_read_ref, taps_read)]
-        steps = step_buf[pl.ds(at_row, props * BLOCK), :] + bias
+        for i in range(props):
+            read_buf[pl.ds(at_row + i * BLOCK, BLOCK), :] = read_new[i]
+        steps = step_buf[pl.ds(at_row, rows_of), :] + bias
         steps = jnp.maximum(steps, 0.0) + jnp.log1p(jnp.exp(-jnp.abs(steps)))
         step = [steps[i * BLOCK : (i + 1) * BLOCK] for i in range(props)]
         cums = []
         for i in range(props):
             cums.append(rate * step[i] + (cums[-1] if cums else 0.0))
         coefs = []
-        where_of = {}
-        for i in range(props):
-            for j in range(i + 1):
-                score = jnp.sum(read_new[i] * write_new[j], axis=-1, keepdims=True)
-                c = jnp.exp(cums[i] - cums[j]) * step[j] * score
-                if i == j:
-                    c = c + skip
-                where_of[(i, j)] = len(coefs)
-                coefs.append(c)
-        first_cum = len(coefs)
+        for i, j in pairs_of:
+            score = jnp.sum(read_new[i] * write_new[j], axis=-1, keepdims=True)
+            c = jnp.exp(cums[i] - cums[j]) * step[j] * score
+            coefs.append(c + skip if i == j else c)
         coefs += [jnp.exp(c) for c in cums]
         high, low = split_of(jnp.concatenate(coefs, axis=0))
-        wide = jnp.dot(
+        wide_buf[r] = jnp.dot(
             jnp.concatenate([high, low], axis=1), expand, preferred_element_type=f32
         )
 
+    def carry_over(first):
+        span = CARRY * rows_of
+        at_row = first * rows_of
+        asked = jnp.transpose(read_buf[at_row : at_row + span, :])
+        col = lax.broadcasted_iota(jnp.int32, asked.shape, 1)
+        seq_of = col // rows_of * BLOCK + col % BLOCK
+        total = None
+        for s in range(0, CARRY * BLOCK, 2):
+            at = first * BLOCK + s
+            lhs = jnp.concatenate([half_ref[at + e] for e in range(2)], axis=1)
+            rhs = jnp.concatenate(
+                [jnp.where(seq_of == s + e, asked, 0.0).astype(bf16) for e in range(2)], axis=0
+            )
+            got = jnp.dot(lhs, rhs, preferred_element_type=f32)
+            total = got if total is None else total + got
+        carried_buf[at_row : at_row + span, :] = jnp.transpose(total)
+
+    def finish_rows(r):
+        at_row = pl.multiple_of(r * rows_of, rows_of)
+
         def at(e):
-            return wide[e * BLOCK : (e + 1) * BLOCK]
-
-        read_all = jnp.concatenate(read_new, axis=0)
-        carried = None
-        for s in range(0, BLOCK, 2):
-            lhs = jnp.concatenate(
-                [jnp.where(row_r == s + e, read_all, 0.0).astype(bf16) for e in range(2)], axis=1
-            )
-            rhs = jnp.concatenate([half_ref[at_seq + s + e] for e in range(2)], axis=1)
-            got = lax.dot_general(lhs, rhs, nt, preferred_element_type=f32)
-            carried = got if carried is None else carried + got
+            return wide_buf[r, e * BLOCK : (e + 1) * BLOCK, :]
+
+        def part(buf, i):
+            return buf[pl.ds(at_row + i * BLOCK, BLOCK), :]
+
         squares = jnp.zeros((BLOCK, 128), f32)
         outs = []
         for i in range(props):
-            y = at(first_cum + i) * carried[i * BLOCK : (i + 1) * BLOCK]
+            y = at(first_cum + i) * part(carried_buf, i)
             for j in range(i + 1):
-                y = y + at(where_of[(i, j)]) * inner_new[j]
-            g = y * silu_of(gate_buf[pl.ds(at_row + i * BLOCK, BLOCK), :])
+                y = y + at(pairs_of[(i, j)]) * part(inner_buf, j)
+            g = y * silu_of(part(gate_buf, i))
             squares = jnp.where(lane_of == i, jnp.sum(g * g, axis=-1, keepdims=True), squares)
             outs.append(g * gain)
         sq_ref[r] = squares
-        un_buf[pl.ds(at_row, props * BLOCK), :] = jnp.concatenate(outs, axis=0).astype(bf16)
-        return carry
-
-    lax.fori_loop(0, blocks, block, 0)
+        un_buf[pl.ds(at_row, rows_of), :] = jnp.concatenate(outs, axis=0).astype(bf16)
+
+    def each(fn, lo, hi, step):
+        def run(i, carry):
+            for u in range(step):
+                fn(lo + i * step + u)
+            return carry
+
+        lax.fori_loop(0, (hi - lo) // step, run, 0)
+
+    each(prepare, 0, blocks, 2)
+    for first in range(0, blocks, CARRY):
+        carry_over(first)
+    each(finish_rows, 0, blocks, 2)
     un = un_buf[...]
     wide_tile = 512
     for lo in range(0, outw_ref.shape[1], wide_tile):
@@ -1062,6 +1130,8 @@
     tokens = rows.shape[0]
     width = weights[-1].shape[1]
     ranks = seqs // BLOCK
+    props = tokens // seqs
+    coefs = props * (props + 1) // 2 + props
     f32, bf16 = jnp.float32, jnp.bfloat16
     vmem = pl.BlockSpec(memory_space=pltpu.VMEM)
     shape = jax.ShapeDtypeStruct
@@ -1081,11 +1151,13 @@
             pltpu.VMEM((tokens, states), f32),
             pltpu.VMEM((tokens, weights[3].shape[0]), f32),
             pltpu.VMEM((tokens, cols), bf16),
+            pltpu.VMEM((tokens, cols), f32),
+            pltpu.VMEM((ranks, coefs * BLOCK, cols), f32),
             pltpu.SemaphoreType.DMA((ranks,)),
         ],
         compiler_params=pltpu.CompilerParams(vmem_limit_bytes=8 * 1024 * 1024),
         name="core",
-    )(rank, rows, kept(base, pltpu.VMEM), kept(half, pltpu.VMEM), *parts, *weights, bias, decay_log, skip, ci, cw, cr, gain)
+    )(rank, rows, kept(base, pltpu.VMEM), kept(half, pltpu.VMEM), *parts, *[kept(w, pltpu.VMEM) for w in weights], bias, decay_log, skip, ci, cw, cr, gain)
 
 
 def tail_kernel(
@@ -1298,6 +1370,7 @@
         conv_write,
         conv_read,
         saved_state.reshape(seqs, heads * head_dim, states),
+        weights,
     )
     rows, base, half = got[:3]
     partial_value, squares, base_state = core(
@@ -1307,7 +1380,7 @@
         base,
         half,
         got[3:6],
-        weights,
+        got[6:],
         row(step_bias),
         row(decay_log),
         row(skip_gain),

time: 47.9 us -> 43.1 us (0.90)
  Pallas kernels: 46.1 us -> 41.5 us
    pallas_call x1, Pallas kernels: 21.7 us -> 17.9 us  [lead(): pl.pallas_call(functools.partial(lead_kernel, n), out_shape=[shape((n, 2,...]
    pallas_call x1, Pallas kernels: 8.21 us -> 7.4 us  [core(): pl.pallas_call(functools.partial(core_kernel, heads), out_shape=[shape((t...]
where the time goes in v2:
time: 43.1 us; the launch traced here: 42.9 us
  Pallas kernels  41.5 us (96%)
  between operations  0.78 us (2%)
  local copies, waits for them, and re-layouts  0.69 us (2%)
    pallas_call x1, Pallas kernels, lead(): pl.pallas_call(functools.partial(lead_kernel, n), out_shape=[shape((n, 2,...  17.9 us
    pallas_call x1, Pallas kernels, finish(): pl.pallas_call(functools.partial(tail_kernel, n, channels), out_shape=jax...  16.2 us
    pallas_call x1, Pallas kernels, core(): pl.pallas_call(functools.partial(core_kernel, heads), out_shape=[shape((t...  7.4 us

profile of v2, /device:TPU:0, one launch (start us, length us, event | category | flops | bytes accessed | tf_op | source)
XLA Modules:
  0.0 42.9 jit_solution(11725607634028245648)
XLA Ops:
  0.6 0.0 copy-start
  0.7 0.0 copy-start.1
  0.7 0.0 copy-start.2
  0.7 0.0 copy-start.3
  0.7 0.0 copy-start.4
  0.7 0.0 copy-start.5
  0.7 0.0 copy-start.6
  0.7 17.9 %lead.1 = (bf16[4,2,32,2048]{3,2,1,0:T(8,128)(2,1)S(1)}, f32[64,512,128]{2,1,0:T(8,128)S(1)}, bf16[64,512,128]{2,1,0:T(8,128)(2,1)S(1)}, f32[3,64,512]{2,1,0:T(8...) custom-call(bf16[32,2048]{1,0:T(8,128)(2,1)} %tokens_hbm.1, ...), custom_call_target="tpu_custom_call" | custom-call | tf_op jit(solution)/shard_map/lead/pallas_call | solution.py:913
  18.6 0.0 copy-done
  18.6 0.0 copy-done.1
  18.6 0.0 copy-done.2
  18.6 0.0 copy-done.3
  18.6 0.0 copy-done.4
  18.7 0.0 copy-done.5
  18.7 0.0 copy-done.6
  18.7 7.4 %core.1 = (bf16[256,2048]{1,0:T(8,128)(2,1)S(1)}, f32[8,8,128]{2,1,0:T(8,128)S(1)}, f32[64,512,128]{2,1,0:T(8,128)}) custom-call(s32[1]{0:T(128)} %bitcast.rank_ref, bf16[256,2048]{1,0:T(8,128)(2,1)S(1)} %bitcast.16, f32[64,512,128]{2,1,0:T(8,128)S(1)} %get-tuple-element.18.base_ref, bf16[64,512,128]{2,1,0:T(8,128)(2,1)S(1)} %get-tuple-element.19.half_ref, ...), custom_call_target="tpu_custom_call" | custom-call | tf_op jit(solution)/shard_map/core/pallas_call | solution.py:1138
  26.1 16.2 %tail.1 = bf16[32,2048]{1,0:T(8,128)(2,1)S(1)} custom-call(bf16[4,2,32,2048]{3,2,1,0:T(8,128)(2,1)S(1)} %bitcast.17, f32[8,8,128]{2,1,0:T(8,128)S(1)} %get-tuple-element.30.sq), custom_call_target="tpu_custom_call" | custom-call | tf_op jit(solution)/shard_map/tail/pallas_call | solution.py:1307
  42.3 0.7 %copy.24 = bf16[32,2048]{1,0:T(8,128)(2,1)} copy(bf16[32,2048]{1,0:T(8,128)(2,1)S(1)} %tail.1) | data formatting | bytes 262144
Async XLA Ops:
  0.6 18.0 %copy-start = (bf16[4,4096]{1,0:T(4,128)(2,1)S(1)}, bf16[4,4096]{1,0:T(4,128)(2,1)}, u32[]{:S(2)}) copy-start(bf16[4,4096]{1,0:T(4,128)(2,1)} %taps_inner_ref.1) | copy-start | bytes 98308
  0.7 18.0 %copy-start.1 = (bf16[4,1024]{1,0:T(4,128)(2,1)S(1)}, bf16[4,1024]{1,0:T(4,128)(2,1)}, u32[]{:S(2)}) copy-start(bf16[4,1024]{1,0:T(4,128)(2,1)} %taps_write_ref.1) | copy-start | bytes 24580
  0.7 18.0 %copy-start.2 = (bf16[4,1024]{1,0:T(4,128)(2,1)S(1)}, bf16[4,1024]{1,0:T(4,128)(2,1)}, u32[]{:S(2)}) copy-start(bf16[4,1024]{1,0:T(4,128)(2,1)} %taps_read_ref.1) | copy-start | bytes 24580
  0.7 18.0 %copy-start.3 = (f32[4096]{0:T(1024)S(1)}, f32[4096]{0:T(1024)}, u32[]{:S(2)}) copy-start(f32[4096]{0:T(1024)} %param.34) | copy-start | bytes 49156
  0.7 18.0 %copy-start.4 = (f32[64]{0:T(128)S(1)}, f32[64]{0:T(128)}, u32[]{:S(2)}) copy-start(f32[64]{0:T(128)} %param.29) | copy-start | bytes 772
  0.7 18.0 %copy-start.5 = (f32[64]{0:T(128)S(1)}, f32[64]{0:T(128)}, u32[]{:S(2)}) copy-start(f32[64]{0:T(128)} %param.28) | copy-start | bytes 772
  0.7 18.0 %copy-start.6 = (f32[64]{0:T(128)S(1)}, f32[64]{0:T(128)}, u32[]{:S(2)}) copy-start(f32[64]{0:T(128)} %param.30) | copy-start | bytes 772

commit v3 on v2

--- a/solution.py
+++ b/solution.py
@@ -941,6 +941,76 @@
     )(*[kept(x, pltpu.HBM) for x in small + (state,) + weights])
 
 
+def carry_over(first, props, half_ref, read_ref, carried_ref):
+    rows_of = props * BLOCK
+    span = CARRY * rows_of
+    asked = jnp.transpose(read_ref[pl.ds(pl.multiple_of(first * rows_of, span), span), :])
+    col = lax.broadcasted_iota(jnp.int32, asked.shape, 1)
+    seq_of = col // rows_of * BLOCK + col % BLOCK
+    total = None
+    for s in range(0, CARRY * BLOCK, 2):
+        lhs = jnp.concatenate([half_ref[first * BLOCK + s + e] for e in range(2)], axis=1)
+        rhs = jnp.concatenate(
+            [jnp.where(seq_of == s + e, asked, 0.0).astype(jnp.bfloat16) for e in range(2)], axis=0
+        )
+        got = jnp.dot(lhs, rhs, preferred_element_type=jnp.float32)
+        total = got if total is None else total + got
+    carried_ref[...] = jnp.transpose(total)
+
+
+def mix_rows(first, props, gain, wide_ref, inner_ref, gate_ref, carried_ref, un_ref, put_square):
+    rows_of = props * BLOCK
+    pairs_of = pairs_up_to(props)
+    lane_of = lax.broadcasted_iota(jnp.int32, (BLOCK, 128), 1)
+
+    def one(b):
+        r = first + b
+        near = pl.multiple_of(b * rows_of, rows_of)
+        at_row = pl.multiple_of(r * rows_of, rows_of)
+
+        def at(e):
+            return wide_ref[r, e * BLOCK : (e + 1) * BLOCK, :]
+
+        def part(ref, i):
+            return ref[pl.ds(at_row + i * BLOCK, BLOCK), :]
+
+        squares = jnp.zeros((BLOCK, 128), jnp.float32)
+        outs = []
+        for i in range(props):
+            y = at(len(pairs_of) + i) * carried_ref[pl.ds(near + i * BLOCK, BLOCK), :]
+            for j in range(i + 1):
+                y = y + at(pairs_of[(i, j)]) * part(inner_ref, j)
+            g = y * silu_of(part(gate_ref, i))
+            squares = jnp.where(lane_of == i, jnp.sum(g * g, axis=-1, keepdims=True), squares)
+            outs.append(g * gain)
+        put_square(b, squares)
+        un_ref[pl.ds(near, rows_of), :] = jnp.concatenate(outs, axis=0).astype(jnp.bfloat16)
+
+    each(one, 0, CARRY, 2)
+
+
+def each(fn, lo, hi, step):
+    def run(i, carry):
+        for u in range(step):
+            fn(lo + i * step + u)
+        return carry
+
+    lax.fori_loop(0, (hi - lo) // step, run, 0)
+
+
+def pairs_up_to(props):
+    order = [(i, j) for i in range(props) for j in range(i + 1)]
+    return {p: e for e, p in enumerate(order)}
+
+
+def out_tiles(un_ref, outw_ref, put):
+    un = un_ref[...]
+    tile = 512
+    for lo in range(0, outw_ref.shape[1], tile):
+        got = jnp.dot(un, outw_ref[:, lo : lo + tile], preferred_element_type=jnp.float32)
+        put(pl.ds(lo, tile), got.astype(jnp.bfloat16))
+
+
 def core_kernel(
     heads,
     rank_ref,
@@ -968,12 +1038,12 @@
     state_out,
     gate_buf,
     inner_buf,
+    read_buf,
+    wide_buf,
     write_buf,
-    read_buf,
     step_buf,
     un_buf,
     carried_buf,
-    wide_buf,
     sems,
 ):
     f32, bf16 = jnp.float32, jnp.bfloat16
@@ -1016,14 +1086,9 @@
     expand = jnp.where(
         lane // (cols // heads) + rank * heads == row % head_count, 1.0, 0.0
     ).astype(bf16)
-    lane_of = lax.broadcasted_iota(jnp.int32, (BLOCK, 128), 1)
 
     rows_of = props * BLOCK
-    pairs_of = {}
-    for i in range(props):
-        for j in range(i + 1):
-            pairs_of[(i, j)] = len(pairs_of)
-    first_cum = len(pairs_of)
+    pairs_of = pairs_up_to(props)
 
     def prepare(r):
         at_row = pl.multiple_of(r * rows_of, rows_of)
@@ -1065,62 +1130,21 @@
             jnp.concatenate([high, low], axis=1), expand, preferred_element_type=f32
         )
 
-    def carry_over(first):
-        span = CARRY * rows_of
-        at_row = first * rows_of
-        asked = jnp.transpose(read_buf[at_row : at_row + span, :])
-        col = lax.broadcasted_iota(jnp.int32, asked.shape, 1)
-        seq_of = col // rows_of * BLOCK + col % BLOCK
-        total = None
-        for s in range(0, CARRY * BLOCK, 2):
-            at = first * BLOCK + s
-            lhs = jnp.concatenate([half_ref[at + e] for e in range(2)], axis=1)
-            rhs = jnp.concatenate(
-                [jnp.where(seq_of == s + e, asked, 0.0).astype(bf16) for e in range(2)], axis=0
-            )
-            got = jnp.dot(lhs, rhs, preferred_element_type=f32)
-            total = got if total is None else total + got
-        carried_buf[at_row : at_row + span, :] = jnp.transpose(total)
-
-    def finish_rows(r):
-        at_row = pl.multiple_of(r * rows_of, rows_of)
-
-        def at(e):
-            return wide_buf[r, e * BLOCK : (e + 1) * BLOCK, :]
-
-        def part(buf, i):
-            return buf[pl.ds(at_row + i * BLOCK, BLOCK), :]
-
-        squares = jnp.zeros((BLOCK, 128), f32)
-        outs = []
-        for i in range(props):
-            y = at(first_cum + i) * part(carried_buf, i)
-            for j in range(i + 1):
-                y = y + at(pairs_of[(i, j)]) * part(inner_buf, j)
-            g = y * silu_of(part(gate_buf, i))
-            squares = jnp.where(lane_of == i, jnp.sum(g * g, axis=-1, keepdims=True), squares)
-            outs.append(g * gain)
-        sq_ref[r] = squares
-        un_buf[pl.ds(at_row, rows_of), :] = jnp.concatenate(outs, axis=0).astype(bf16)
-
-    def each(fn, lo, hi, step):
-        def run(i, carry):
-            for u in range(step):
-                fn(lo + i * step + u)
-            return carry
-
-        lax.fori_loop(0, (hi - lo) // step, run, 0)
-
     each(prepare, 0, blocks, 2)
-    for first in range(0, blocks, CARRY):
-        carry_over(first)
-    each(finish_rows, 0, blocks, 2)
-    un = un_buf[...]
-    wide_tile = 512
-    for lo in range(0, outw_ref.shape[1], wide_tile):
-        out_ref[:, lo : lo + wide_tile] = jnp.dot(
-            un, outw_ref[:, lo : lo + wide_tile], preferred_element_type=f32
-        ).astype(bf16)
+    first = jnp.where(rank < blocks // 2, CARRY, 0)
+
+    def put_square(e, squares):
+        sq_ref[e] = squares
+
+    carry_over(first, props, half_ref, read_buf, carried_buf)
+    mix_rows(
+        first, props, gain, wide_buf, inner_buf, gate_buf, carried_buf, un_buf, put_square
+    )
+
+    def put(cut, got):
+        out_ref[:, cut] = got
+
+    out_tiles(un_buf, outw_ref, put)
     for b in range(blocks):
         flush(b).wait()
 
@@ -1135,24 +1159,25 @@
     f32, bf16 = jnp.float32, jnp.bfloat16
     vmem = pl.BlockSpec(memory_space=pltpu.VMEM)
     shape = jax.ShapeDtypeStruct
+    kept_in = pltpu.VMEM
     return pl.pallas_call(
         functools.partial(core_kernel, heads),
         out_shape=[
-            shape((tokens, width), bf16),
-            shape((ranks, BLOCK, 128), f32),
+            kept_in((tokens // 2, width), bf16),
+            kept_in((ranks // 2, BLOCK, 128), f32),
             pltpu.HBM(base.shape, f32),
+            kept_in((tokens, cols), f32),
+            kept_in((tokens, cols), f32),
+            kept_in((tokens, states), f32),
+            kept_in((ranks, coefs * BLOCK, cols), f32),
         ],
         in_specs=[pl.BlockSpec(memory_space=pltpu.SMEM)] + [vmem] * 19,
-        out_specs=[vmem, vmem, pl.BlockSpec(memory_space=pl.ANY)],
+        out_specs=[vmem, vmem, pl.BlockSpec(memory_space=pl.ANY)] + [vmem] * 4,
         scratch_shapes=[
-            pltpu.VMEM((tokens, cols), f32),
-            pltpu.VMEM((tokens, cols), f32),
-            pltpu.VMEM((tokens, states), f32),
             pltpu.VMEM((tokens, states), f32),
             pltpu.VMEM((tokens, weights[3].shape[0]), f32),
-            pltpu.VMEM((tokens, cols), bf16),
-            pltpu.VMEM((tokens, cols), f32),
-            pltpu.VMEM((ranks, coefs * BLOCK, cols), f32),
+            pltpu.VMEM((tokens // 2, cols), bf16),
+            pltpu.VMEM((tokens // 2, cols), f32),
             pltpu.SemaphoreType.DMA((ranks,)),
         ],
         compiler_params=pltpu.CompilerParams(vmem_limit_bytes=8 * 1024 * 1024),
@@ -1161,130 +1186,225 @@
 
 
 def tail_kernel(
-    n, channels, part, sq, mixed, sqs, out, turned, pbuf, rbuf, lbuf, rout, lout, ps, pr, rs, rr, ls, lr, ss, sr
+    n,
+    props,
+    channels,
+    far,
+    far_sq,
+    gate,
+    inner,
+    read,
+    wide,
+    half,
+    outw,
+    gain_ref,
+    mixed,
+    near,
+    near_sq,
+    carried,
+    un,
+    out,
+    out_sq,
+    pbuf,
+    rbuf,
+    lbuf,
+    rout,
+    lout,
+    psq,
+    rsq,
+    lsq,
+    routq,
+    loutq,
+    ps,
+    pr,
+    rs,
+    rr,
+    ls,
+    lr,
 ):
     f32 = jnp.float32
     k = lax.axis_index("kv")
     t = lax.axis_index("tp")
     rank = k * 2 + t
-    ranks = n * 2
+    mid = n // 2
     right = {"kv": lax.rem(k + 1, n)}
     left = {"kv": lax.rem(k + n - 1, n)}
     partner = {"tp": 1 - t}
-    span = part.shape[3] // CHUNKS
+    span = far.shape[3] // CHUNKS
+    rows = far.shape[2]
     barrier = pltpu.get_barrier_semaphore()
 
-    def peer(o):
-        p = lax.rem(rank + o, ranks)
-        return {"kv": p // 2, "tp": lax.rem(p, 2)}
-
-    for o in range(1, ranks):
-        pl.semaphore_signal(barrier, inc=1, device_id=peer(o), device_id_type=MESH)
-    pl.semaphore_wait(barrier, ranks - 1)
-
-    def cut(c):
-        return pl.ds(c * span, span)
-
-    def across(j, c):
-        return remote(
-            part.at[j, 1 - t, :, cut(c)], pbuf.at[j, :, cut(c)], ps.at[j, c], pr.at[j, c], partner
-        )
+    low = k < mid
+    first = jnp.where(low, 0, CARRY)
+    inside = (k > 0) & (k < n - 1)
+    pl.semaphore_signal(barrier, inc=1, device_id=partner, device_id_type=MESH)
+
+    @pl.when(k < n - 1)
+    def _():
+        pl.semaphore_signal(barrier, inc=1, device_id=right, device_id_type=MESH)
+
+    @pl.when(k > 0)
+    def _():
+        pl.semaphore_signal(barrier, inc=1, device_id=left, device_id_type=MESH)
+
+    @pl.when(inside)
+    def _():
+        pl.semaphore_wait(barrier, 3)
+
+    @pl.when(jnp.logical_not(inside))
+    def _():
+        pl.semaphore_wait(barrier, 2)
+
+    pieces = range(CHUNKS + 1)
+
+    def piece(data, squares, lead, c):
+        if c == CHUNKS:
+            return squares.at[lead]
+        return data.at[(*lead, slice(None), pl.ds(c * span, span))]
+
+    def across(away, i, c):
+        at = jnp.where(low, mid - 1 - i, i)
+        j = jnp.where(low, (mid if away else 0) + at, at + (0 if away else mid))
+        lead = (at, 1 - t)
+        src = piece(far, far_sq, lead, c) if away else piece(near, near_sq, lead, c)
+        return remote(src, piece(pbuf, psq, (j,), c), ps.at[j, c], pr.at[j, c], partner)
+
+    def arrived(j, c):
+        there = piece(pbuf, psq, (j,), c)
+        return remote(there, there, ps.at[j, c], pr.at[j, c], partner)
 
     def to_right(d, c):
-        return remote(
-            rout.at[d, :, cut(c)], rbuf.at[d, :, cut(c)], rs.at[d, c], rr.at[d, c], right
-        )
+        src, dst = piece(rout, routq, (d,), c), piece(rbuf, rsq, (d,), c)
+        return remote(src, dst, rs.at[d, c], rr.at[d, c], right)
 
     def to_left(d, c):
-        return remote(lout.at[d, :, cut(c)], lbuf.at[d, :, cut(c)], ls.at[d, c], lr.at[d, c], left)
-
-    def square(o):
-        p = lax.rem(rank + o, ranks)
-        return remote(sq.at[p], sqs.at[rank], ss.at[o], sr.at[o], peer(o))
-
-    low = k < n // 2
-    for i in range(n):
-        j = jnp.where(low, n - 1 - i, i)
-        for c in range(CHUNKS):
-            across(j, c).start()
-    for o in range(1, ranks):
-        square(o).start()
-    sqs[rank] = sq[rank]
-
-    def pair(j, c):
-        across(j, c).wait_recv()
-        return part[j, t, :, cut(c)].astype(f32) + pbuf[j, :, cut(c)].astype(f32)
-
-    def rightward():
+        src, dst = piece(lout, loutq, (d,), c), piece(lbuf, lsq, (d,), c)
+        return remote(src, dst, ls.at[d, c], lr.at[d, c], left)
+
+    for i in range(mid):
+        for c in pieces:
+            across(True, i, c).start()
+
+
+    def read_of(data, squares, lead, c):
+        return piece(data, squares, lead, c)[...].astype(f32)
+
+    def pair(away, at, j, c):
+        arrived(j, c).wait_recv()
+        lead = (at, t)
+        own = read_of(far, far_sq, lead, c) if away else read_of(near, near_sq, lead, c)
+        return own + read_of(pbuf, psq, (j,), c)
+
+    def pair_low(j, c):
+        return pair(j >= mid, j % mid, j, c)
+
+    def pair_high(j, c):
+        return pair(j < mid, j % mid, j, c)
+
+    def send_right(value, d, c):
+        ref = piece(rout, routq, (d,), c)
+        ref[...] = value.astype(ref.dtype)
+        to_right(d, c).start()
+
+    def send_left(value, d, c):
+        ref = piece(lout, loutq, (d,), c)
+        ref[...] = value.astype(ref.dtype)
+        to_left(d, c).start()
+
+    @pl.when(k == 0)
+    def _():
+        for d in range(n - 1, mid - 1, -1):
+            for c in pieces:
+                send_right(pair_low(d, c), d, c)
+
+    @pl.when(k == n - 1)
+    def _():
+        for d in range(mid):
+            for c in pieces:
+                send_left(pair_high(d, c), d, c)
+
+    def put_square(e, squares):
+        near_sq[lax.div(e, 2), lax.rem(e, 2)] = squares
+
+    carry_over(first, props, half, read, carried)
+    gain = own_slice(gain_ref, rank * gate.shape[1], gate.shape[1])
+    mix_rows(first, props, gain, wide, inner, gate, carried, un, put_square)
+    def put(at, got):
+        for j in range(mid):
+            for side in range(2):
+                lo = (j * 2 + side) * rows
+                near[j, side, :, at] = got[lo : lo + rows]
+
+    out_tiles(un, outw, put)
+    for i in range(mid):
+        for c in pieces:
+            across(False, i, c).start()
+
+    def rightward(pair_of, skip):
         for d in range(n - 1, 0, -1):
-            for c in range(CHUNKS):
-                @pl.when((k < d) & (k == 0))
-                def _():
-                    rout[d, :, cut(c)] = pair(d, c).astype(rout.dtype)
-                    to_right(d, c).start()
+            for c in pieces:
+                if d < skip:
+                    @pl.when(k == 0)
+                    def _():
+                        send_right(pair_of(d, c), d, c)
 
                 @pl.when((k < d) & (k > 0))
                 def _():
-                    value = pair(d, c)
+                    value = pair_of(d, c)
                     to_right(d, c).wait_recv()
-                    rout[d, :, cut(c)] = (value + rbuf[d, :, cut(c)].astype(f32)).astype(rout.dtype)
-                    to_right(d, c).start()
-
-    def leftward():
+                    send_right(value + read_of(rbuf, rsq, (d,), c), d, c)
+
+    def leftward(pair_of, skip):
         for d in range(n - 1):
-            for c in range(CHUNKS):
-                @pl.when((k > d) & (k == n - 1))
-                def _():
-                    lout[d, :, cut(c)] = pair(d, c).astype(lout.dtype)
-                    to_left(d, c).start()
+            for c in pieces:
+                if d >= skip:
+                    @pl.when(k == n - 1)
+                    def _():
+                        send_left(pair_of(d, c), d, c)
 
                 @pl.when((k > d) & (k < n - 1))
                 def _():
-                    value = pair(d, c)
+                    value = pair_of(d, c)
                     to_left(d, c).wait_recv()
-                    lout[d, :, cut(c)] = (value + lbuf[d, :, cut(c)].astype(f32)).astype(lout.dtype)
-                    to_left(d, c).start()
-
-    @pl.when(k < n // 2)
-    def _():
-        rightward()
-        leftward()
-
-    @pl.when(k >= n // 2)
-    def _():
-        leftward()
-        rightward()
-
-    for c in range(CHUNKS):
-        out[:, cut(c)] = pair(k, c)
+                    send_left(value + read_of(lbuf, lsq, (d,), c), d, c)
+
+    def total(at, c):
+        ref = out_sq if c == CHUNKS else out.at[:, pl.ds(c * span, span)]
+        ref[...] = pair(False, at, k, c)
 
         @pl.when(k > 0)
         def _():
             to_right(k, c).wait_recv()
-            out[:, cut(c)] += rbuf[k, :, cut(c)].astype(f32)
+            ref[...] += read_of(rbuf, rsq, (k,), c)
 
         @pl.when(k < n - 1)
         def _():
             to_left(k, c).wait_recv()
-            out[:, cut(c)] += lbuf[k, :, cut(c)].astype(f32)
-
-    for o in range(1, ranks):
-        square(o).wait_send()
-        source = lax.rem(rank + ranks - o, ranks)
-        remote(sq.at[rank], sqs.at[source], ss.at[o], sr.at[o], peer(o)).wait_recv()
-    scale = lax.rsqrt(jnp.sum(sqs[...], axis=0) / channels + EPSILON)
-    props = out.shape[0] // BLOCK
+            ref[...] += read_of(lbuf, lsq, (k,), c)
+
+    @pl.when(low)
+    def _():
+        rightward(pair_low, mid)
+        leftward(pair_low, mid)
+
+    @pl.when(jnp.logical_not(low))
+    def _():
+        leftward(pair_high, mid)
+        rightward(pair_high, mid)
+
+    for c in pieces:
+        total(k - jnp.where(low, 0, mid), c)
+    scale = lax.rsqrt(out_sq[...] / channels + EPSILON)
     for i in range(props):
-        rows = out[i * BLOCK : (i + 1) * BLOCK, :] * scale[:, i : i + 1]
-        turned[i * BLOCK : (i + 1) * BLOCK, :] = rows
+        out[i * BLOCK : (i + 1) * BLOCK, :] = (
+            out[i * BLOCK : (i + 1) * BLOCK, :] * scale[:, i : i + 1]
+        )
     mixed[...] = jnp.dot(
-        turn_rows(out.shape[0], props, True),
-        turned[...].astype(mixed.dtype),
-        preferred_element_type=f32,
+        turn_rows(rows, props, True), out[...].astype(mixed.dtype), preferred_element_type=f32
     ).astype(mixed.dtype)
     for j in range(n):
-        for c in range(CHUNKS):
-            across(j, c).wait_send()
+        for c in pieces:
+            arrived(j, c).wait_send()
 
             @pl.when(k < j)
             def _():
@@ -1295,33 +1415,38 @@
                 to_left(j, c).wait_send()
 
 
-def finish(partial_value, squares, channels):
+def finish(far, squares, near, half, outw, gain, props, channels):
     n = lax.axis_size("kv")
     ranks = n * 2
-    rows = partial_value.shape[0] // ranks
-    cols = partial_value.shape[1]
+    tokens, cols = near[0].shape
+    rows = tokens // ranks
+    width = far.shape[1]
     dma = pltpu.SemaphoreType.DMA
     vmem = pl.BlockSpec(memory_space=pltpu.VMEM)
-    kind = partial_value.dtype
+    kind = far.dtype
     f32 = jnp.float32
+    refs = [far.reshape(n // 2, 2, rows, width), squares.reshape(n // 2, 2, BLOCK, 128), *near, half, outw]
     return pl.pallas_call(
-        functools.partial(tail_kernel, n, channels),
-        out_shape=jax.ShapeDtypeStruct((rows, cols), kind),
-        in_specs=[vmem, vmem],
+        functools.partial(tail_kernel, n, props, channels),
+        out_shape=jax.ShapeDtypeStruct((rows, width), kind),
+        in_specs=[vmem] * (len(refs) + 1),
         out_specs=vmem,
         scratch_shapes=[
-            pltpu.VMEM(squares.shape, f32),
-            pltpu.VMEM((rows, cols), f32),
-            pltpu.VMEM((rows, cols), f32),
+            pltpu.VMEM((n // 2, 2, rows, width), kind),
+            pltpu.VMEM((n // 2, 2, BLOCK, 128), f32),
+            pltpu.VMEM((tokens // 2, cols), f32),
+            pltpu.VMEM((tokens // 2, cols), kind),
+            pltpu.VMEM((rows, width), f32),
+            pltpu.VMEM((BLOCK, 128), f32),
         ]
-        + [pltpu.VMEM((n, rows, cols), kind)] * 5
-        + [dma((n, CHUNKS))] * 6
-        + [dma((ranks,))] * 2,
+        + [pltpu.VMEM((n, rows, width), kind)] * 5
+        + [pltpu.VMEM((n, BLOCK, 128), f32)] * 5
+        + [dma((n, CHUNKS + 1))] * 6,
         compiler_params=pltpu.CompilerParams(
-            collective_id=3, has_side_effects=True, vmem_limit_bytes=32 * 1024 * 1024
+            collective_id=3, has_side_effects=True, vmem_limit_bytes=12 * 1024 * 1024
         ),
         name="tail",
-    )(partial_value.reshape(n, 2, rows, cols), squares)
+    )(*[kept(x, pltpu.VMEM) for x in refs], gain)
 
 
 def whole_groups(tokens, saved_state, last_steps):
@@ -1373,7 +1498,7 @@
         weights,
     )
     rows, base, half = got[:3]
-    partial_value, squares, base_state = core(
+    far, squares, base_state, *near = core(
         device_rank.reshape(1).astype(jnp.int32),
         heads,
         rows.reshape(-1, rows.shape[-1]),
@@ -1389,7 +1514,9 @@
         conv_read,
         row(out_gain),
     )
-    mixed = finish(partial_value, squares, out_gain.shape[0])
+    mixed = finish(
+        far, squares, near, half, got[-1], row(out_gain), last_steps.shape[1], out_gain.shape[0]
+    )
     return (mixed, base_state.reshape(saved_state.shape))
 
 

time: 43.1 us -> 41 us (0.951)
  Pallas kernels: 41.5 us -> 39.4 us
    pallas_call x2, Pallas kernels: 23.6 us -> 21.5 us  [the longest x1 14.6 us: finish(): pl.pallas_call(functools.partial(tail_kernel, n, props, channels), out_sh...]
where the time goes in v3:
time: 41 us; the launch traced here: 40.9 us
  Pallas kernels  39.4 us (96%)
  between operations  0.78 us (2%)
  local copies, waits for them, and re-layouts  0.69 us (2%)
    pallas_call x1, Pallas kernels, lead(): pl.pallas_call(functools.partial(lead_kernel, n), out_shape=[shape((n, 2,...  17.9 us
    pallas_call x1, Pallas kernels, finish(): pl.pallas_call(functools.partial(tail_kernel, n, props, channels), out_sh...  14.6 us
    pallas_call x1, Pallas kernels, core(): pl.pallas_call(functools.partial(core_kernel, heads), out_shape=[kept_in(...  6.87 us

profile of v3, /device:TPU:0, one launch (start us, length us, event | category | flops | bytes accessed | tf_op | source)
XLA Modules:
  0.0 40.9 jit_solution(12641001022849494154)
XLA Ops:
  0.6 0.0 copy-start
  0.7 0.0 copy-start.1
  0.7 0.0 copy-start.2
  0.7 0.0 copy-start.3
  0.7 0.0 copy-start.4
  0.7 0.0 copy-start.5
  0.7 0.0 copy-start.6
  0.7 17.9 %lead.1 = (bf16[4,2,32,2048]{3,2,1,0:T(8,128)(2,1)S(1)}, f32[64,512,128]{2,1,0:T(8,128)S(1)}, bf16[64,512,128]{2,1,0:T(8,128)(2,1)S(1)}, f32[3,64,512]{2,1,0:T(8...) custom-call(bf16[32,2048]{1,0:T(8,128)(2,1)} %tokens_hbm.1, ...), custom_call_target="tpu_custom_call" | custom-call | tf_op jit(solution)/shard_map/lead/pallas_call | solution.py:913
  18.6 0.0 copy-done
  18.6 0.0 copy-done.1
  18.6 0.0 copy-done.2
  18.6 0.0 copy-done.3
  18.6 0.0 copy-done.4
  18.7 0.0 copy-done.5
  18.7 0.0 copy-done.6
  18.7 6.9 %core.1 = (bf16[128,2048]{1,0:T(8,128)(2,1)S(1)}, f32[4,8,128]{2,1,0:T(8,128)S(1)}, f32[64,512,128]{2,1,0:T(8,128)}, f32[256,512]{1,0:T(8,128)S(1)}, f32[256,512...) custom-call(s32[1]{0:T(128)} %bitcast.rank_ref, bf16[256,2048]{1,0:T(8,128)(2,1)S(1)} %bitcast.17, ...), custom_call_target="tpu_custom_call" | custom-call | tf_op jit(solution)/shard_map/core/pallas_call | solution.py:1163
  25.6 14.6 %tail.1 = bf16[32,2048]{1,0:T(8,128)(2,1)S(1)} custom-call(bf16[2,2,32,2048]{3,2,1,0:T(8,128)(2,1)S(1)} %bitcast.18, f32[2,2,8,128]{3,2,1,0:T(8,128)S(1)} %bitcast.21, f32[256,512]{1,0:T(8,128)S(1)} %get-tuple-element.35.gate, f32[256,512]{1,0:T(8,128)S(1)} %get-tuple-element.36.inner, f32[256,128]{1,0:T(8,128)S(1)} %get-tuple-element.37.read, ...), custom_call_target="tpu_custom_call" | custom-call | tf_op jit(solution)/shard_map/tail/pallas_call | solution.py:1429
  40.2 0.7 %copy.24 = bf16[32,2048]{1,0:T(8,128)(2,1)} copy(bf16[32,2048]{1,0:T(8,128)(2,1)S(1)} %tail.1) | data formatting | bytes 262144
Async XLA Ops:
  0.6 18.0 %copy-start = (bf16[4,4096]{1,0:T(4,128)(2,1)S(1)}, bf16[4,4096]{1,0:T(4,128)(2,1)}, u32[]{:S(2)}) copy-start(bf16[4,4096]{1,0:T(4,128)(2,1)} %taps_inner_ref.1) | copy-start | bytes 98308
  0.7 18.0 %copy-start.1 = (f32[4096]{0:T(1024)S(1)}, f32[4096]{0:T(1024)}, u32[]{:S(2)}) copy-start(f32[4096]{0:T(1024)} %param.34) | copy-start | bytes 49156
  0.7 18.0 %copy-start.2 = (bf16[4,1024]{1,0:T(4,128)(2,1)S(1)}, bf16[4,1024]{1,0:T(4,128)(2,1)}, u32[]{:S(2)}) copy-start(bf16[4,1024]{1,0:T(4,128)(2,1)} %taps_write_ref.1) | copy-start | bytes 24580
  0.7 18.0 %copy-start.3 = (bf16[4,1024]{1,0:T(4,128)(2,1)S(1)}, bf16[4,1024]{1,0:T(4,128)(2,1)}, u32[]{:S(2)}) copy-start(bf16[4,1024]{1,0:T(4,128)(2,1)} %taps_read_ref.1) | copy-start | bytes 24580
  0.7 18.0 %copy-start.4 = (f32[64]{0:T(128)S(1)}, f32[64]{0:T(128)}, u32[]{:S(2)}) copy-start(f32[64]{0:T(128)} %param.29) | copy-start | bytes 772
  0.7 18.0 %copy-start.5 = (f32[64]{0:T(128)S(1)}, f32[64]{0:T(128)}, u32[]{:S(2)}) copy-start(f32[64]{0:T(128)} %param.28) | copy-start | bytes 772
  0.7 18.0 %copy-start.6 = (f32[64]{0:T(128)S(1)}, f32[64]{0:T(128)}, u32[]{:S(2)}) copy-start(f32[64]{0:T(128)} %param.30) | copy-start | bytes 772

commit v4 on v3

--- a/solution.py
+++ b/solution.py
@@ -517,7 +517,9 @@
 
 AHEAD = 3
 CARRY = 4
-HOPS_AT = (0, 1, 1, 2, 3, 4, 5, 6)
+HOPS_IN = (1, 2, 3, 4, 5, 6, 6, 6)
+HOPS_END = (0, 0, 0, 1, 2, 3, 4, 6)
+SPLITS = 2
 
 
 def pick(x, rows, first):
@@ -537,7 +539,8 @@
 
 
 def silu_of(x):
-    return x / (1.0 + jnp.exp(-x))
+    half = 0.5 * x
+    return half + half * jnp.tanh(half)
 
 
 def round_of(x):
@@ -697,7 +700,7 @@
     def _():
         pl.semaphore_wait(barrier, 2)
 
-    span = own_ref.shape[1] // CHUNKS
+    span = own_ref.shape[1] // SPLITS
 
     def view(j, c):
         return rows_ref.at[j, t, :, pl.ds(c * span, span)]
@@ -746,7 +749,7 @@
             def _():
                 across(k + s, c).start()
 
-    for c in range(CHUNKS):
+    for c in range(SPLITS):
         hop(0, c)
     local = pltpu.make_async_copy(own_ref, rows_ref.at[k, t], local_sem)
     local.start()
@@ -859,8 +862,8 @@
                 base_ref[s, lo:hi, :] = new
                 half_ref[s, lo:hi, :] = new.astype(bf16)
 
-    hops = [(s, c) for s in range(1, n) for c in range(CHUNKS)]
-    done = 0
+    hops = [(s, c) for s in range(1, n) for c in range(SPLITS)]
+    done = [0, 0]
     for part in range(2):
         prepare(part)
         for g in range(per_half):
@@ -870,15 +873,19 @@
             for c in more:
                 c.start()
             update(part, g * BLOCK, BLOCK)
-            goal = len(hops) * HOPS_AT[b] // 6
-            while done < goal:
-                hop(*hops[done])
-                done += 1
+            for ends, plan in enumerate((HOPS_IN, HOPS_END)):
+                goal = len(hops) * plan[b] // 6
+                if done[ends] < goal:
+                    @pl.when(jnp.logical_not(inside) if ends else inside)
+                    def _():
+                        for e in range(done[ends], goal):
+                            hop(*hops[e])
+                    done[ends] = goal
     for w in weights:
         w.wait()
     local.wait()
     for s in range(n - 1):
-        for c in range(CHUNKS):
+        for c in range(SPLITS):
             @pl.when((k - s >= 0) & (k < n - 1))
             def _():
                 to_right(s, c).wait_send()
@@ -887,7 +894,7 @@
             def _():
                 to_left(s, c).wait_send()
     for j in range(n):
-        for c in range(CHUNKS):
+        for c in range(SPLITS):
             across(j, c).wait_send()
             there = rows_ref.at[j, 1 - t, :, pl.ds(c * span, span)]
             remote(there, there, fs.at[j, c], fr.at[j, c], partner).wait_recv()
@@ -930,8 +937,8 @@
             pltpu.VMEM((2, cols, half_rows), bf16),
             pltpu.VMEM((2, half_rows, states), bf16),
         ]
-        + [dma((n - 1, CHUNKS))] * 4
-        + [dma((n, CHUNKS))] * 2
+        + [dma((n - 1, SPLITS))] * 4
+        + [dma((n, SPLITS))] * 2
         + [dma, dma((blocks,)), dma((len(small),)), dma((len(weights),))]
         + [pltpu.VMEM(x.shape, x.dtype) for x in small],
         compiler_params=pltpu.CompilerParams(
@@ -1058,8 +1065,6 @@
         span = pl.ds(b * BLOCK, BLOCK)
         return pltpu.make_async_copy(base_ref.at[span], state_out.at[span], sems.at[b])
 
-    for b in range(blocks):
-        flush(b).start()
     rows = rows_ref[...]
     tile = 256
     for w_ref, buf in ((inner_ref, inner_buf), (gate_ref, gate_buf)):
@@ -1130,6 +1135,8 @@
             jnp.concatenate([high, low], axis=1), expand, preferred_element_type=f32
         )
 
+    for b in range(blocks):
+        flush(b).start()
     each(prepare, 0, blocks, 2)
     first = jnp.where(rank < blocks // 2, CARRY, 0)
 

time: 41 us -> 40.1 us (0.978)
  Pallas kernels: 39.4 us -> 38.4 us
    pallas_call x1, Pallas kernels: 17.9 us -> 17 us  [lead(): pl.pallas_call(functools.partial(lead_kernel, n), out_shape=[shape((n, 2,...]
    pallas_call x1, Pallas kernels: 6.87 us -> 6.13 us  [core(): pl.pallas_call(functools.partial(core_kernel, heads), out_shape=[kept_in(...]
    pallas_call x1, Pallas kernels: 14.6 us -> 15.3 us  [finish(): pl.pallas_call(functools.partial(tail_kernel, n, props, channels), out_sh...]
where the time goes in v4:
time: 40.1 us; the launch traced here: 39.9 us
  Pallas kernels  38.4 us (96%)
  between operations  0.78 us (2%)
  local copies, waits for them, and re-layouts  0.69 us (2%)
    pallas_call x1, Pallas kernels, lead(): pl.pallas_call(functools.partial(lead_kernel, n), out_shape=[shape((n, 2,...  17 us
    pallas_call x1, Pallas kernels, finish(): pl.pallas_call(functools.partial(tail_kernel, n, props, channels), out_sh...  15.3 us
    pallas_call x1, Pallas kernels, core(): pl.pallas_call(functools.partial(core_kernel, heads), out_shape=[kept_in(...  6.13 us

profile of v4, /device:TPU:0, one launch (start us, length us, event | category | flops | bytes accessed | tf_op | source)
XLA Modules:
  0.0 39.9 jit_solution(7645183180171403282)
XLA Ops:
  0.6 0.0 copy-start
  0.7 0.0 copy-start.1
  0.7 0.0 copy-start.2
  0.7 0.0 copy-start.3
  0.7 0.0 copy-start.4
  0.7 0.0 copy-start.5
  0.7 0.0 copy-start.6
  0.7 17.0 %lead.1 = (bf16[4,2,32,2048]{3,2,1,0:T(8,128)(2,1)S(1)}, f32[64,512,128]{2,1,0:T(8,128)S(1)}, bf16[64,512,128]{2,1,0:T(8,128)(2,1)S(1)}, f32[3,64,512]{2,1,0:T(8...) custom-call(bf16[32,2048]{1,0:T(8,128)(2,1)} %tokens_hbm.1, ...), custom_call_target="tpu_custom_call" | custom-call | tf_op jit(solution)/shard_map/lead/pallas_call | solution.py:920
  17.7 0.0 copy-done
  17.7 0.0 copy-done.1
  17.7 0.0 copy-done.2
  17.7 0.0 copy-done.3
  17.7 0.0 copy-done.4
  17.8 0.0 copy-done.5
  17.8 0.0 copy-done.6
  17.8 6.1 %core.1 = (bf16[128,2048]{1,0:T(8,128)(2,1)S(1)}, f32[4,8,128]{2,1,0:T(8,128)S(1)}, f32[64,512,128]{2,1,0:T(8,128)}, f32[256,512]{1,0:T(8,128)S(1)}, f32[256,512...) custom-call(s32[1]{0:T(128)} %bitcast.rank_ref, bf16[256,2048]{1,0:T(8,128)(2,1)S(1)} %bitcast.17, ...), custom_call_target="tpu_custom_call" | custom-call | tf_op jit(solution)/shard_map/core/pallas_call | solution.py:1170
  23.9 15.3 %tail.1 = bf16[32,2048]{1,0:T(8,128)(2,1)S(1)} custom-call(bf16[2,2,32,2048]{3,2,1,0:T(8,128)(2,1)S(1)} %bitcast.18, f32[2,2,8,128]{3,2,1,0:T(8,128)S(1)} %bitcast.21, f32[256,512]{1,0:T(8,128)S(1)} %get-tuple-element.35.gate, f32[256,512]{1,0:T(8,128)S(1)} %get-tuple-element.36.inner, f32[256,128]{1,0:T(8,128)S(1)} %get-tuple-element.37.read, ...), custom_call_target="tpu_custom_call" | custom-call | tf_op jit(solution)/shard_map/tail/pallas_call | solution.py:1436
  39.3 0.7 %copy.24 = bf16[32,2048]{1,0:T(8,128)(2,1)} copy(bf16[32,2048]{1,0:T(8,128)(2,1)S(1)} %tail.1) | data formatting | bytes 262144
Async XLA Ops:
  0.6 17.1 %copy-start = (bf16[4,4096]{1,0:T(4,128)(2,1)S(1)}, bf16[4,4096]{1,0:T(4,128)(2,1)}, u32[]{:S(2)}) copy-start(bf16[4,4096]{1,0:T(4,128)(2,1)} %taps_inner_ref.1) | copy-start | bytes 98308
  0.7 17.1 %copy-start.1 = (f32[4096]{0:T(1024)S(1)}, f32[4096]{0:T(1024)}, u32[]{:S(2)}) copy-start(f32[4096]{0:T(1024)} %param.34) | copy-start | bytes 49156
  0.7 17.1 %copy-start.2 = (bf16[4,1024]{1,0:T(4,128)(2,1)S(1)}, bf16[4,1024]{1,0:T(4,128)(2,1)}, u32[]{:S(2)}) copy-start(bf16[4,1024]{1,0:T(4,128)(2,1)} %taps_write_ref.1) | copy-start | bytes 24580
  0.7 17.1 %copy-start.3 = (bf16[4,1024]{1,0:T(4,128)(2,1)S(1)}, bf16[4,1024]{1,0:T(4,128)(2,1)}, u32[]{:S(2)}) copy-start(bf16[4,1024]{1,0:T(4,128)(2,1)} %taps_read_ref.1) | copy-start | bytes 24580
  0.7 17.1 %copy-start.4 = (f32[64]{0:T(128)S(1)}, f32[64]{0:T(128)}, u32[]{:S(2)}) copy-start(f32[64]{0:T(128)} %param.29) | copy-start | bytes 772
  0.7 17.1 %copy-start.5 = (f32[64]{0:T(128)S(1)}, f32[64]{0:T(128)}, u32[]{:S(2)}) copy-start(f32[64]{0:T(128)} %param.28) | copy-start | bytes 772
  0.7 17.1 %copy-start.6 = (f32[64]{0:T(128)S(1)}, f32[64]{0:T(128)}, u32[]{:S(2)}) copy-start(f32[64]{0:T(128)} %param.30) | copy-start | bytes 772
